TPU v7x, 32 devices: a whole 2x2x4 slice. The times are simulated.
32 devices in a mesh: grp: 2 (over y), dp: 2 (over x), kv: 4 (over z), tp: 2 (over core).
Axes of the slice: x: 2, y: 2, z: 4, core: 2. Of those that a mesh axis runs over, the one named last changes fastest.
Arguments:
- tokens: bfloat16 [256, 4, 4096], P(('grp', 'dp'), None, ('kv', 'tp')), parts along dimension 0, may hold values from -160 to 160
- norm_gain: float32 [4096], replicated, may hold values from 0.1 to 1.9
- w_query: bfloat16 [4096, 16, 64], P(None, 'kv'), may hold values from -0.09375 to 0.09375
- w_key: bfloat16 [4096, 16, 64], P(None, 'kv'), may hold values from -0.09375 to 0.09375
- w_value: bfloat16 [4096, 16, 128], P(None, 'kv', 'tp'), may hold values from -0.09375 to 0.09375
- w_outgate: bfloat16 [4096, 16, 128], P(None, 'kv', 'tp'), may hold values from -0.09375 to 0.09375
- w_input: bfloat16 [4096, 16], replicated, may hold values from -0.09375 to 0.09375
- w_forget: bfloat16 [4096, 16], replicated, may hold values from -0.09375 to 0.09375
- forget_bias: float32 [16], replicated, may hold values from -1 to 4
- head_gain: float32 [16, 128], replicated, may hold values from 0.1 to 1.9
- w_out: bfloat16 [16, 128, 4096], P('kv', 'tp'), may hold values from -0.125 to 0.125
- memory: float32 [256, 16, 128, 64], P(('grp', 'dp'), 'kv', 'tp'), parts along dimension 0, may hold values from -12 to 12
- normalizer: float32 [256, 16, 64], P(('grp', 'dp'), 'kv'), parts along dimension 0, may hold values from -12 to 12
- stabilizer: float32 [256, 16], P(('grp', 'dp'), 'kv'), parts along dimension 0, may hold values from -1 to 1
- prev_keys: bfloat16 [256, 4, 16, 64], P(('grp', 'dp'), None, 'kv'), parts along dimension 0, may hold values from -6 to 6
- prev_values: bfloat16 [256, 4, 16, 128], P(('grp', 'dp'), None, 'kv', 'tp'), parts along dimension 0, may hold values from -6 to 6
- prev_input: float32 [256, 4, 16], P(('grp', 'dp'), None, 'kv'), parts along dimension 0, may hold values from -4 to 4
- prev_forget: float32 [256, 4, 16], P(('grp', 'dp'), None, 'kv'), parts along dimension 0, may hold values from -2 to -0.02
- accepted: int32 [256], P(('grp', 'dp')), parts along dimension 0, may hold values from 0 to 4
Outputs:
- mixed: bfloat16 [256, 4, 4096], P(('grp', 'dp'), None, ('kv', 'tp')), parts along dimension 0
- new_memory: float32 [256, 16, 128, 64], P(('grp', 'dp'), 'kv', 'tp'), parts along dimension 0
- new_normalizer: float32 [256, 16, 64], P(('grp', 'dp'), 'kv'), parts along dimension 0
- new_stabilizer: float32 [256, 16], P(('grp', 'dp'), 'kv'), parts along dimension 0
- new_keys: bfloat16 [256, 4, 16, 64], P(('grp', 'dp'), None, 'kv'), parts along dimension 0
- new_values: bfloat16 [256, 4, 16, 128], P(('grp', 'dp'), None, 'kv', 'tp'), parts along dimension 0
- new_input: float32 [256, 4, 16], P(('grp', 'dp'), None, 'kv'), parts along dimension 0
- new_forget: float32 [256, 4, 16], P(('grp', 'dp'), None, 'kv'), parts along dimension 0
There are 2 independent parts, one for each index of `grp`. A program takes and returns all parts, laid end to end along the dimension named above; an argument that names none is the same for every part. Nothing has to cross between parts.
All inputs are finite; a program needn't handle non-finite values.
Results may differ from a plain program's by a relative error of at most 0.038.
Values may be sent and summed in bfloat16 or wider, within the bound.
A program may use at most 128 MiB of HBM per device.

v0:
```python
import functools
import jax
import jax.numpy as jnp
from jax import lax
from jax.sharding import PartitionSpec as P
from jax.experimental import pallas as pl
from jax.experimental.pallas import tpu as pltpu

EPS = 1e-06
FAR_NEGATIVE = -1e30
HIGHEST = lax.Precision.HIGHEST
MESH = pl.DeviceIdType.MESH
F32 = jnp.float32
BF16 = jnp.bfloat16
VMEM_LIMIT = 60 << 20


def nn(a, b, precision=None):
    return lax.dot_general(
        a, b, (((1,), (0,)), ((), ())), precision=precision, preferred_element_type=F32
    )


def nt(a, b, precision=None):
    return lax.dot_general(
        a, b, (((1,), (1,)), ((), ())), precision=precision, preferred_element_type=F32
    )


def enter(n, z, c):
    barrier = pltpu.get_barrier_semaphore()
    pl.semaphore_signal(barrier, inc=1, device_id={"tp": 1 - c}, device_id_type=MESH)

    @pl.when(z > 0)
    def _():
        pl.semaphore_signal(barrier, inc=1, device_id={"kv": z - 1}, device_id_type=MESH)

    @pl.when(z < n - 1)
    def _():
        pl.semaphore_signal(barrier, inc=1, device_id={"kv": z + 1}, device_id_type=MESH)

    peers = 1 + (z > 0).astype(jnp.int32) + (z < n - 1).astype(jnp.int32)
    pl.semaphore_wait(barrier, peers)


def project_kernel(
    n, key_size, halves,
    x_ref, gain_ref, wq_hbm, wk_hbm, wv_hbm, wo_hbm, wi_hbm, wf_hbm, bias_ref, pk_ref, pv_ref, out_hbm,
    q_out, k_out, v_out, og_out, gi_out, gf_out, pk_out, pv_out, wout_out,
    xg, weights, acc, squares,
    load_sem, send_sem, recv_sem, wsend_sem, wrecv_sem,
):
    z = lax.axis_index("kv")
    c = lax.axis_index("tp")
    width = x_ref.shape[2]
    rows = x_ref.shape[0] * x_ref.shape[1]
    height = rows // halves
    loads, spans, at = [], [], 0
    for i, src in enumerate((wq_hbm, wk_hbm, wv_hbm, wo_hbm, wi_hbm, wf_hbm)):
        size = src.shape[0]
        spans.append(slice(at, at + size))
        loads.append(
            pltpu.make_async_copy(src, weights.at[pl.ds(at, size)], load_sem.at[i])
        )
        at += size
    for load in loads:
        load.start()
    mine = 2 * z + c
    flat = x_ref[...].reshape(rows, width)
    for half in range(halves):
        xg[mine, half] = flat[half * height : (half + 1) * height]
    acc[...] = jnp.zeros_like(acc)
    squares[...] = jnp.zeros_like(squares)
    enter(n, z, c)

    def hop(slot, half, way, target):
        return pltpu.make_async_remote_copy(
            src_ref=xg.at[slot, half], dst_ref=xg.at[slot, half],
            send_sem=send_sem.at[way, slot, half], recv_sem=recv_sem.at[slot, half],
            device_id=target, device_id_type=MESH,
        )

    up, down, side = {"kv": z + 1}, {"kv": z - 1}, {"tp": 1 - c}

    for half in range(halves):
        @pl.when(z < n - 1)
        def _():
            hop(mine, half, 0, up).start()

        @pl.when(z > 0)
        def _():
            hop(mine, half, 1, down).start()

        hop(mine, half, 2, side).start()


    def out_piece(i):
        col = pl.multiple_of((2 * i + 1 - c) * width, width)
        return pltpu.make_async_remote_copy(
            src_ref=out_hbm.at[:, pl.ds(col, width)],
            dst_ref=wout_out.at[i],
            send_sem=wsend_sem.at[i], recv_sem=wrecv_sem.at[i],
            device_id=side, device_id_type=MESH,
        )

    for i in range(n):
        out_piece(i).start()
    heads, values = pv_ref.shape[2:]
    old_keys = pk_ref[...].astype(F32).reshape(rows, heads, key_size)
    old_values = pv_ref[...].astype(F32).reshape(rows, heads, values)
    for h in range(heads):
        pk_out[:, h * key_size : (h + 1) * key_size] = old_keys[:, h, :].astype(BF16)
        pv_out[h * values : (h + 1) * values, :] = old_values[:, h, :].T.astype(BF16)
    for load in loads:
        load.wait()

    def process(slot):
        cols = pl.ds(pl.multiple_of(slot * width, width), width)
        x = jnp.concatenate([xg[slot, half] for half in range(halves)], axis=0).astype(F32)
        square = x * x
        total = squares[...]
        for i in range(width // 128):
            total = total + square[:, i * 128 : (i + 1) * 128]
        squares[...] = total
        acc[...] += nt(weights[:, cols], (x * gain_ref[:, cols]).astype(BF16))

    def process_owner(owner):
        process(2 * owner + c)
        slot = 2 * owner + 1 - c
        for half in range(halves):
            hop(slot, half, 2, side).wait_recv()
        process(slot)

    def forward(k, half):
        @pl.when(z - k >= 0)
        def _():
            slot = 2 * (z - k) + c
            hop(slot, half, 0, up).wait_recv()

            @pl.when(z < n - 1)
            def _():
                hop(slot, half, 0, up).start()

            hop(slot, half, 2, side).start()

        @pl.when(z + k <= n - 1)
        def _():
            slot = 2 * (z + k) + c
            hop(slot, half, 1, down).wait_recv()

            @pl.when(z > 0)
            def _():
                hop(slot, half, 1, down).start()

            hop(slot, half, 2, side).start()

    def step(k, carry):
        for half in range(halves - 1):
            forward(k, half)

        @pl.when(z - (k - 1) >= 0)
        def _():
            process_owner(z - (k - 1))

        forward(k, halves - 1)

        @pl.when((z + k - 1 <= n - 1) & (k > 1))
        def _():
            process_owner(z + k - 1)

        return carry

    lax.fori_loop(1, n + 1, step, 0)

    depth = gain_ref.shape[1]
    total = nt(jnp.ones((8, 128), F32), squares[...], HIGHEST)
    inv = lax.rsqrt(total[0:1] / depth + EPS)
    q, k, v, og, gi, gf = [acc[part, :] * inv for part in spans]
    q_out[...] = (q.astype(BF16).astype(F32) * key_size ** (-0.5)).astype(BF16)
    k_out[...] = k.T.astype(BF16)
    v_out[...] = v.astype(BF16)
    og_out[...] = og
    all_heads = gf.shape[0]
    diagonal = lax.broadcasted_iota(jnp.int32, (all_heads, all_heads), 0) == (
        lax.broadcasted_iota(jnp.int32, (all_heads, all_heads), 1)
    )
    shift = nn(jnp.where(diagonal, bias_ref[...], 0.0), jnp.ones(gf.shape, F32), HIGHEST)
    raw = gf + shift
    gf = jnp.minimum(raw, 0.0) - jnp.log1p(jnp.exp(-jnp.abs(raw)))
    local_heads = gi_out.shape[0]
    for values, out in ((gi, gi_out), (gf, gf_out)):
        total = values[:local_heads]
        for i in range(1, n):
            total = jnp.where(z == i, values[i * local_heads : (i + 1) * local_heads], total)
        out[...] = total

    for i in range(n):
        out_piece(i).wait()

    def drain(i, carry):
        slot = 2 * i + c
        for half in range(halves):
            @pl.when((i <= z) & (z < n - 1))
            def _():
                hop(slot, half, 0, up).wait_send()

            @pl.when((i >= z) & (z > 0))
            def _():
                hop(slot, half, 1, down).wait_send()

            hop(slot, half, 2, side).wait_send()
        return carry

    lax.fori_loop(0, n, drain, 0)


def recurrent_kernel(
    q_ref, k_ref, v_ref, og_ref, gi_ref, gf_ref, pk_ref, pv_ref, pi_ref, pf_ref,
    acc_ref, stab_ref, nrm_ref, gain_ref, mem_ref,
    nm_ref, nn_ref, ns_ref, ni_ref, nf_ref, g_ref, sq_ref,
    vts, kps, dfull, wexp, ro,
):
    step = pl.program_id(0)
    steps = pl.num_programs(0)
    block, heads, values, keys = mem_ref.shape
    span, _, seqs = pi_ref.shape
    rows = seqs * span
    lanes = 128
    iota = lambda shape, d: lax.broadcasted_iota(jnp.int32, shape, d)

    @pl.when(step == 0)
    def _():
        spread = (iota((seqs, rows), 0) == iota((seqs, rows), 1) // span)
        expand = spread.astype(F32)
        lane_pos = iota((span, rows), 1) % span == iota((span, rows), 0)
        dropped = iota((span, seqs), 0) >= acc_ref[...]
        ro[...] = jnp.zeros_like(ro)
        single = [
            jnp.where(lane_pos, ref[h : h + 1, :], 0.0)
            for h in range(heads)
            for ref in (gi_ref, gf_ref)
        ]
        compact = nt(jnp.concatenate(single, axis=0), expand, HIGHEST)
        position = iota((2 * span, seqs), 0)
        stack, decays = [], []
        for h in range(heads):
            stab = stab_ref[h : h + 1, :]
            f = jnp.where(dropped, 0.0, pf_ref[:, h, :])
            i = jnp.where(dropped, FAR_NEGATIVE, pi_ref[:, h, :])
            new_i = compact[2 * h * span : (2 * h + 1) * span]
            new_f = compact[(2 * h + 1) * span : (2 * h + 2) * span]
            ni_ref[:, h, :] = new_i
            nf_ref[:, h, :] = new_f
            total = []
            for j in range(span):
                total.append(f[j : j + 1] + total[-1] if total else f[0:1])
            e = total[-1]
            for j in range(span):
                total.append(total[-1] + new_f[j : j + 1])
            run_prev = jnp.concatenate(total[:span], axis=0)
            run_all = jnp.concatenate(total, axis=0)
            in_all = jnp.concatenate([i, new_i], axis=0)
            u = e - run_prev + i
            ns = jnp.maximum(e + stab, jnp.max(u, axis=0, keepdims=True))
            ns_ref[h : h + 1, :] = ns
            decays.append(jnp.exp(e + stab - ns))
            stack += [jnp.exp(u - ns), jnp.zeros((8 - span, seqs), F32)]
            for t in range(span):
                latest = total[span + t]
                d = jnp.where(position <= span + t, latest - run_all + in_all, FAR_NEGATIVE)
                g = latest + stab
                top = jnp.maximum(jnp.max(d, axis=0, keepdims=True), g)
                pad = jnp.zeros((16 - 2 * span - 2, seqs), F32)
                stack += [jnp.exp(d - top), jnp.exp(g - top), jnp.exp(-top), pad]
        wide = nn(jnp.concatenate(stack, axis=0), expand, HIGHEST)
        decays = jnp.concatenate(decays + [jnp.zeros((8 - heads, seqs), F32)], axis=0).T
        each = 8 + 16 * span
        for h in range(heads):
            base = h * each
            share_row = jnp.sum(
                jnp.where(lane_pos, wide[base : base + span], 0.0), axis=0, keepdims=True
            )
            old = pk_ref[:, h * keys : (h + 1) * keys]
            odd = (iota((rows, keys), 0) // span) % 2
            kps[h] = jnp.concatenate(
                [jnp.where(odd == p, old, jnp.zeros_like(old)) for p in range(2)], axis=1
            )
            part = slice(h * values, (h + 1) * values)
            vts[part, :] = (pv_ref[part, :].astype(F32) * share_row).astype(BF16)
            full = jnp.broadcast_to(decays[:, h : h + 1], (seqs, keys))
            dfull[h] = full
            mixed = jnp.where(spread, share_row, 0.0).astype(BF16)
            nn_ref[:, h, :] = full * nrm_ref[:, h, :] + nn(mixed, old)
            gathered = jnp.zeros((16, rows), F32)
            for t in range(span):
                at = base + 8 + 16 * t
                gathered = jnp.where(
                    iota((16, rows), 1) % span == t, wide[at : at + 16], gathered
                )
            wexp[h] = gathered

    first = step * block
    start = pl.multiple_of((first * span) // lanes * lanes, lanes)
    half = pl.ds(start, lanes)
    pair = ((iota((values, lanes), 1) + start) // span - first) // 2
    parity = (iota((keys, lanes), 1) // span) % 2
    for h in range(heads):
        part = slice(h * values, (h + 1) * values)
        memory = [mem_ref[s, h] for s in range(block)]
        packed = jnp.concatenate(
            [
                jnp.concatenate([memory[s].astype(BF16), memory[s + 1].astype(BF16)], axis=1)
                for s in range(0, block, 2)
            ],
            axis=0,
        )
        query = q_ref[h * keys : (h + 1) * keys, half]
        none = jnp.zeros_like(query)
        both = jnp.concatenate([jnp.where(parity == p, query, none) for p in range(2)], axis=0)
        read = nn(packed, both)
        total = ro[part, half]
        for s in range(block // 2):
            total = jnp.where(pair == s, read[s * values : (s + 1) * values], total)
        ro[part, half] = total
        shared = vts[part, half]
        zero = jnp.zeros_like(shared)
        left = jnp.concatenate(
            [jnp.where(pair == s, shared, zero) for s in range(block // 2)], axis=0
        )
        update = nn(left, kps[h, half, :])
        for s in range(block):
            at = s // 2 * values
            nm_ref[s, h] = (
                dfull[h, pl.ds(first + s, 1), :] * memory[s]
                + update[at : at + values, s % 2 * keys : (s % 2 + 1) * keys]
            )

    @pl.when(step == steps - 1)
    def _():
        same = iota((rows, rows), 0) // span == iota((rows, rows), 1) // span
        spread = iota((seqs, rows), 0) == iota((seqs, rows), 1) // span
        q = q_ref[...]
        owner = iota(q.shape, 0) // keys

        z = lax.axis_index("kv")
        gains = gain_ref[:, :values]
        for i in range(1, gain_ref.shape[1] // values):
            gains = jnp.where(
                lax.axis_index("tp") == i, gain_ref[:, i * values : (i + 1) * values], gains
            )
        local = gains[:heads]
        for i in range(1, gain_ref.shape[0] // heads):
            local = jnp.where(z == i, gains[i * heads : (i + 1) * heads], local)

        columns = jnp.concatenate([local, jnp.zeros((8 - heads, values), F32)], axis=0).T

        def tile(w):
            w = jnp.concatenate([w] * (8 // span), axis=0)
            return jnp.broadcast_to(w[None], (rows // 8, 8, rows)).reshape(rows, rows)

        for h in range(heads):
            part = slice(h * values, (h + 1) * values)
            only = jnp.where(owner == h, q, jnp.zeros_like(q))
            w = wexp[h]
            w_prev = jnp.where(same, tile(w[:span]) * nn(pk_ref[...], only), 0.0)
            w_new = jnp.where(same, tile(w[span : 2 * span]) * nn(k_ref[...], only), 0.0)
            carry = w[2 * span : 2 * span + 1]
            floor = w[2 * span + 1 : 2 * span + 2]
            top = nn(pv_ref[part, :], w_prev.astype(BF16)) + nn(v_ref[part, :], w_new.astype(BF16))
            top = top + carry * ro[part, :]
            nq = nn(nrm_ref[:, h, :].astype(BF16), q_ref[h * keys : (h + 1) * keys, :])
            nq = jnp.sum(jnp.where(spread, nq, 0.0), axis=0, keepdims=True)
            under = jnp.sum(w_prev + w_new, axis=0, keepdims=True) + carry * nq
            cell = top / jnp.maximum(jnp.abs(under), floor)
            sq_ref[h : h + 1, :] = jnp.sum(cell * cell, axis=0, keepdims=True)
            gain = columns[:, h : h + 1]
            g_ref[part, :] = (jax.nn.sigmoid(og_ref[part, :]) * cell * gain).astype(BF16)


def output_kernel(
    n, full_values, halves,
    g_ref, sq_ref, own_hbm, other_hbm,
    y_ref,
    g_in, sq_in, both, from_low, from_high, to_high, to_low, total, w_ref,
    load_sem,
    side_send, side_recv, up_send, up_recv, down_send, down_recv,
):
    z = lax.axis_index("kv")
    c = lax.axis_index("tp")
    channels = g_ref.shape[0]
    width = y_ref.shape[2]
    loads = []
    for d in range(n):
        col = pl.multiple_of((2 * d + c) * width, width)
        loads += [
            pltpu.make_async_copy(
                own_hbm.at[:, pl.ds(col, width)], w_ref.at[d, pl.ds(0, channels)],
                load_sem.at[2 * d],
            ),
            pltpu.make_async_copy(
                other_hbm.at[d], w_ref.at[d, pl.ds(channels, channels)], load_sem.at[2 * d + 1]
            ),
        ]
    for load in loads:
        load.start()
    enter(n, z, c)
    side = {"tp": 1 - c}
    swaps = [
        pltpu.make_async_remote_copy(
            src_ref=src, dst_ref=dst, send_sem=side_send.at[i], recv_sem=side_recv.at[i],
            device_id=side, device_id_type=MESH,
        )
        for i, (src, dst) in enumerate(((g_ref, g_in), (sq_ref, sq_in)))
    ]
    for swap in swaps:
        swap.start()
    for swap in swaps:
        swap.wait_recv()
    inv = lax.rsqrt((sq_ref[...] + sq_in[...]) / full_values + EPS)
    heads = sq_ref.shape[0]
    values = channels // heads
    for i, src in enumerate((g_ref, g_in)):
        scaled = jnp.concatenate(
            [
                src[h * values : (h + 1) * values, :].astype(F32) * inv[h : h + 1, :]
                for h in range(heads)
            ],
            axis=0,
        )
        both[:, i * channels : (i + 1) * channels] = scaled.T.astype(BF16)

    for load in loads:
        load.wait()
    height = both.shape[0] // halves

    def partial(d, half):
        return nn(both[half * height : (half + 1) * height], w_ref[d])

    def upward(d, half):
        return pltpu.make_async_remote_copy(
            src_ref=to_high.at[d, half], dst_ref=from_low.at[d, half],
            send_sem=up_send.at[d, half], recv_sem=up_recv.at[d, half],
            device_id={"kv": z + 1}, device_id_type=MESH,
        )

    def downward(d, half):
        return pltpu.make_async_remote_copy(
            src_ref=to_low.at[d, half], dst_ref=from_high.at[d, half],
            send_sem=down_send.at[d, half], recv_sem=down_recv.at[d, half],
            device_id={"kv": z - 1}, device_id_type=MESH,
        )

    def step(i, carry):
        high = n - 1 - i + z
        low = i - (n - 1 - z)
        for half in range(halves):
            @pl.when((high > z) & (high <= n - 1))
            def _():
                term = partial(high, half)

                @pl.when(z == 0)
                def _():
                    to_high[high, half] = term.astype(BF16)

                @pl.when(z > 0)
                def _():
                    upward(high, half).wait_recv()
                    to_high[high, half] = (term + from_low[high, half].astype(F32)).astype(BF16)

                upward(high, half).start()

            @pl.when((low < z) & (low >= 0))
            def _():
                term = partial(low, half)

                @pl.when(z == n - 1)
                def _():
                    to_low[low, half] = term.astype(BF16)

                @pl.when(z < n - 1)
                def _():
                    downward(low, half).wait_recv()
                    to_low[low, half] = (term + from_high[low, half].astype(F32)).astype(BF16)

                downward(low, half).start()

        return carry

    lax.fori_loop(0, 2 * n - 2, step, 0)
    for half in range(halves):
        total[half] = partial(z, half)
    for half in range(halves):
        @pl.when(z > 0)
        def _():
            upward(z, half).wait_recv()
            total[half] += from_low[z, half].astype(F32)

        @pl.when(z < n - 1)
        def _():
            downward(z, half).wait_recv()
            total[half] += from_high[z, half].astype(F32)

    seqs, span, width = y_ref.shape
    y_ref[...] = total[...].reshape(seqs, span, width).astype(BF16)

    def drain(i, carry):
        for half in range(halves):
            @pl.when(i > z)
            def _():
                upward(i, half).wait_send()

            @pl.when(i < z)
            def _():
                downward(i, half).wait_send()

        return carry

    lax.fori_loop(0, n, drain, 0)
    for swap in swaps:
        swap.wait_send()


def shards(
    n, tokens, norm_gain, w_query, w_key, w_value, w_outgate, w_input, w_forget, forget_bias,
    head_gain, w_out, memory, normalizer, stabilizer, prev_keys, prev_values, prev_input,
    prev_forget, accepted,
):
    seqs, span, width = tokens.shape
    depth, heads, keys = w_query.shape
    values = w_value.shape[2]
    rows = seqs * span
    hk, hv = heads * keys, heads * values
    all_heads = w_input.shape[1]
    sds = jax.ShapeDtypeStruct
    vm = pl.BlockSpec(memory_space=pltpu.VMEM)
    hbm = pl.BlockSpec(memory_space=pl.ANY)
    flip = lambda w: w.transpose(1, 2, 0).reshape(-1, depth)

    halves = 2
    height = rows // halves
    channels = 2 * hk + 2 * hv + 2 * all_heads
    q, k, v, og, gi, gf, pk, pv, wout = pl.pallas_call(
        functools.partial(project_kernel, n, keys, halves),
        out_shape=[
            sds((hk, rows), BF16), sds((rows, hk), BF16), sds((hv, rows), BF16),
            sds((hv, rows), F32), sds((heads, rows), F32), sds((heads, rows), F32),
            sds((rows, hk), BF16), sds((hv, rows), BF16), sds((n, hv, width), BF16),
        ],
        in_specs=[vm, vm] + [hbm] * 6 + [vm, vm, vm, hbm],
        out_specs=[vm] * 8 + [hbm],
        scratch_shapes=[
            pltpu.VMEM((2 * n, halves, height, width), BF16),
            pltpu.VMEM((channels, depth), BF16),
            pltpu.VMEM((channels, rows), F32),
            pltpu.VMEM((rows, 128), F32),
            pltpu.SemaphoreType.DMA((6,)),
            pltpu.SemaphoreType.DMA((3, 2 * n, halves)),
            pltpu.SemaphoreType.DMA((2 * n, halves)),
            pltpu.SemaphoreType.DMA((n,)),
            pltpu.SemaphoreType.DMA((n,)),
        ],
        compiler_params=pltpu.CompilerParams(
            collective_id=0, has_side_effects=True, vmem_limit_bytes=VMEM_LIMIT
        ),
        name="project",
    )(
        tokens, norm_gain.reshape(1, depth),
        flip(w_query), flip(w_key), flip(w_value), flip(w_outgate),
        w_input.T, w_forget.T, forget_bias.reshape(1, all_heads), prev_keys, prev_values,
        w_out.reshape(hv, -1),
    )

    block = 8
    whole = lambda *shape: pl.BlockSpec(shape, lambda i: (0,) * len(shape))
    tile = pl.BlockSpec((block, heads, values, keys), lambda i: (i, 0, 0, 0))
    new_memory, new_normalizer, ns, ni, nf, g, sq = pl.pallas_call(
        recurrent_kernel,
        grid=(seqs // block,),
        out_shape=[
            sds(memory.shape, F32), sds(normalizer.shape, F32), sds((heads, seqs), F32),
            sds((span, heads, seqs), F32), sds((span, heads, seqs), F32),
            sds((hv, rows), BF16), sds((heads, rows), F32),
        ],
        in_specs=[
            whole(hk, rows), whole(rows, hk), whole(hv, rows), whole(hv, rows),
            whole(heads, rows), whole(heads, rows), whole(rows, hk), whole(hv, rows),
            whole(span, heads, seqs), whole(span, heads, seqs), whole(1, seqs),
            whole(heads, seqs), whole(seqs, heads, keys), whole(*head_gain.shape), tile,
        ],
        out_specs=[
            tile, whole(seqs, heads, keys), whole(heads, seqs), whole(span, heads, seqs),
            whole(span, heads, seqs), whole(hv, rows), whole(heads, rows),
        ],
        scratch_shapes=[
            pltpu.VMEM((hv, rows), BF16), pltpu.VMEM((heads, rows, 2 * keys), BF16),
            pltpu.VMEM((heads, seqs, keys), F32), pltpu.VMEM((heads, 16, rows), F32),
            pltpu.VMEM((hv, rows), F32),
        ],
        compiler_params=pltpu.CompilerParams(vmem_limit_bytes=VMEM_LIMIT),
        name="recurrent",
    )(
        q, k, v, og, gi, gf, pk, pv,
        prev_input.transpose(1, 2, 0), prev_forget.transpose(1, 2, 0),
        accepted.reshape(1, seqs), stabilizer.T, normalizer, head_gain, memory,
    )

    y = pl.pallas_call(
        functools.partial(output_kernel, n, values * 2, halves),
        out_shape=sds(tokens.shape, BF16),
        in_specs=[vm, vm, hbm, hbm],
        out_specs=vm,
        scratch_shapes=[pltpu.VMEM((hv, rows), BF16), pltpu.VMEM((heads, rows), F32)]
        + [pltpu.VMEM((rows, 2 * hv), BF16)]
        + [pltpu.VMEM((n, halves, height, width), BF16)] * 4
        + [pltpu.VMEM((halves, height, width), F32), pltpu.VMEM((n, 2 * hv, width), BF16)]
        + [pltpu.SemaphoreType.DMA((2 * n,))]
        + [pltpu.SemaphoreType.DMA((2,))] * 2
        + [pltpu.SemaphoreType.DMA((n, halves))] * 4,
        compiler_params=pltpu.CompilerParams(
            collective_id=1, has_side_effects=True, vmem_limit_bytes=VMEM_LIMIT
        ),
        name="output",
    )(g, sq, w_out.reshape(hv, -1), wout)

    return (
        y,
        new_memory,
        new_normalizer,
        ns.T,
        k.reshape(seqs, span, heads, keys),
        v.T.reshape(seqs, span, heads, values),
        ni.transpose(2, 0, 1),
        nf.transpose(2, 0, 1),
    )


def solution(mesh):
    return jax.shard_map(
        functools.partial(shards, mesh.shape["kv"]),
        mesh=mesh,
        in_specs=(
            P(("grp", "dp"), None, ("kv", "tp")),
            P(),
            P(None, "kv", None),
            P(None, "kv", None),
            P(None, "kv", "tp"),
            P(None, "kv", "tp"),
            P(),
            P(),
            P(),
            P(),
            P("kv", "tp", None),
            P(("grp", "dp"), "kv", "tp", None),
            P(("grp", "dp"), "kv", None),
            P(("grp", "dp"), "kv"),
            P(("grp", "dp"), None, "kv", None),
            P(("grp", "dp"), None, "kv", "tp"),
            P(("grp", "dp"), None, "kv"),
            P(("grp", "dp"), None, "kv"),
            P(("grp", "dp")),
        ),
        out_specs=(
            P(("grp", "dp"), None, ("kv", "tp")),
            P(("grp", "dp"), "kv", "tp", None),
            P(("grp", "dp"), "kv", None),
            P(("grp", "dp"), "kv"),
            P(("grp", "dp"), None, "kv", None),
            P(("grp", "dp"), None, "kv", "tp"),
            P(("grp", "dp"), None, "kv"),
            P(("grp", "dp"), None, "kv"),
        ),
        check_vma=False,
    )
```

profile of v0, /device:TPU:0, one launch (start us, length us, event | category | flops | bytes accessed | tf_op | source)
XLA Modules:
  0.0 67.5 jit_solution(14932283500795133297)
XLA Ops:
  0.6 28.4 %project.1 = (bf16[256,256]{1,0:T(8,128)(2,1)}, bf16[256,256]{1,0:T(8,128)(2,1)}, bf16[256,256]{1,0:T(8,128)(2,1)}, f32[256,256]{1,0:T(8,128)}, f32[4,256]{1,0:T...) custom-call(bf16[64,4,512]{2,1,0:T(4,128)(2,1)} %x_ref.1, ...), custom_call_target="tpu_custom_call" | custom-call | tf_op jit(solution)/shard_map/project/pallas_call | solution.py:542
  29.1 12.7 %recurrent.1 = (f32[64,4,64,64]{3,2,1,0:T(8,128)}, f32[64,4,64]{2,1,0:T(4,128)}, f32[4,64]{1,0:T(4,128)}, f32[4,4,64]{2,1,0:T(4,128)}, f32[4,4,64]{2,1,0:T(4,128...) custom-call(bf16[256,256]{1,0:T(8,128)(2,1)} %get-tuple-element.24.q_ref, bf16[256,256]{1,0:T(8,128)(2,1)} %get-tuple-element.25.k_ref, ...), custom_call_target="tpu_custom_call" | custom-call | tf_op jit(solution)/shard_map/recurrent/pallas_call | solution.py:576
  41.8 0.0 copy-start.1
  41.8 0.0 copy-start
  41.8 22.0 %output.1 = bf16[64,4,512]{2,1,0:T(4,128)(2,1)} custom-call(bf16[256,256]{1,0:T(8,128)(2,1)} %get-tuple-element.32.g_ref, f32[4,256]{1,0:T(4,128)} %get-tuple-element.33.sq_ref, bf16[256,4096]{1,0:T(8,128)(2,1)} %bitcast.26, bf16[4,256,512]{2,1,0:T(8,128)(2,1)} %get-tuple-element.34.other_hbm), custom_call_target="tpu_custom_call" | custom-call | tf_op jit(solution)/shard_map/output/pallas_call | solution.py:607
  63.9 0.0 copy-done.1
  63.9 0.1 copy.28
  64.0 0.9 %reshape.56 = bf16[64,4,4,64]{3,2,1,0:T(4,128)(2,1)} reshape(bf16[256,256]{1,0:T(8,128)(2,1)S(1)} %copy.28) | data formatting | bytes 262144 | tf_op jit(solution)/shard_map/reshape | solution.py:631
  64.8 0.0 copy-done
  64.8 0.9 %reshape.55 = bf16[64,4,4,64]{3,2,1,0:T(4,128)(2,1)} reshape(bf16[256,256]{1,0:T(8,128)(2,1)S(1)} %copy-done) | data formatting | bytes 262144 | tf_op jit(solution)/shard_map/reshape | solution.py:630
  65.7 1.7 %copy.30 = bf16[64,4,512]{2,1,0:T(4,128)(2,1)} copy(bf16[64,4,512]{2,1,0:T(4,128)(2,1)} %output.1) | data formatting | bytes 524288
Async XLA Ops:
  41.8 22.1 %copy-start.1 = (bf16[256,256]{1,0:T(8,128)(2,1)S(1)}, bf16[256,256]{1,0:T(8,128)(2,1)}, u32[]{:S(2)}) copy-start(bf16[256,256]{1,0:T(8,128)(2,1)} %get-tuple-element.26.v_ref) | copy-start | bytes 393220
  41.8 23.0 %copy-start = (bf16[256,256]{1,0:T(8,128)(2,1)S(1)}, bf16[256,256]{1,0:T(8,128)(2,1)}, u32[]{:S(2)}) copy-start(bf16[256,256]{1,0:T(8,128)(2,1)} %get-tuple-element.25.k_ref) | copy-start | bytes 393220
where the time goes:
time: 67.8 us; the launch traced here: 67.5 us
  Pallas kernels  63.2 us (93%)
  local copies, waits for them, and re-layouts  3.59 us (5%)
  between operations  0.69 us (1%)
    pallas_call x1, Pallas kernels, shards(): pl.pallas_call(functools.partial(project_kernel, n, keys, halves), out_sh...  28.4 us
    pallas_call x1, Pallas kernels, shards(): pl.pallas_call(functools.partial(output_kernel, n, values * 2, halves), o...  22 us
    pallas_call x1, Pallas kernels, shards(): pl.pallas_call(recurrent_kernel, grid=(seqs // block,), out_shape=[sds(me...  12.7 us
    unnamed x5, local copies, waits for them, and re-layouts  1.75 us

commit v1 on v0

v1 whole, which is shorter than its diff:
```python
import functools
import jax
import jax.numpy as jnp
from jax import lax
from jax.sharding import PartitionSpec as P
from jax.experimental import pallas as pl
from jax.experimental.pallas import tpu as pltpu

EPS = 1e-06
FAR_NEGATIVE = -1e30
HIGHEST = lax.Precision.HIGHEST
MESH = pl.DeviceIdType.MESH
F32 = jnp.float32
BF16 = jnp.bfloat16
VMEM_LIMIT = 60 << 20
HALVES = 2
PIECES = 2
BLOCK = 8


def nn(a, b, precision=None):
    return lax.dot_general(
        a, b, (((1,), (0,)), ((), ())), precision=precision, preferred_element_type=F32
    )


def nt(a, b, precision=None):
    return lax.dot_general(
        a, b, (((1,), (1,)), ((), ())), precision=precision, preferred_element_type=F32
    )


def iota(shape, d):
    return lax.broadcasted_iota(jnp.int32, shape, d)


def enter(n, z, c):
    barrier = pltpu.get_barrier_semaphore()
    pl.semaphore_signal(barrier, inc=1, device_id={"tp": 1 - c}, device_id_type=MESH)

    @pl.when(z > 0)
    def _():
        pl.semaphore_signal(barrier, inc=1, device_id={"kv": z - 1}, device_id_type=MESH)

    @pl.when(z < n - 1)
    def _():
        pl.semaphore_signal(barrier, inc=1, device_id={"kv": z + 1}, device_id_type=MESH)

    peers = 1 + (z > 0).astype(jnp.int32) + (z < n - 1).astype(jnp.int32)
    pl.semaphore_wait(barrier, peers)


def fused_kernel(
    n, key_size, full_values,
    x_ref, gain_ref, bias_ref, pk_ref, pv_ref, pi_ref, pf_ref, acc_ref, stab_ref, nrm_ref, hgain_ref,
    wq_hbm, wk_hbm, wv_hbm, wo_hbm, wi_hbm, wf_hbm, mem_hbm, out_hbm,
    y_out, k_out, v_out, vts, kps, dfull, nn_out, ns_out, ni_out, nf_out,
    xg, weights, acc, squares, mem, packed, nrmb, gates, nsrow, g_own, sq_own, g_in, sq_in, both,
    w_ref, from_low, from_high, to_high, to_low, total_ref,
    load_sem, mem_sem, wload_sem, wsend_sem, wrecv_sem,
    send0, recv0, send1, side1, recv1, ex_send, ex_recv, up_send, up_recv, down_send, down_recv,
):
    z = lax.axis_index("kv")
    c = lax.axis_index("tp")
    seqs, span, width = x_ref.shape
    rows = seqs * span
    lanes = rows // HALVES
    piece = lanes // PIECES
    depth = gain_ref.shape[1]
    keys = key_size
    heads, values = pv_ref.shape[2:]
    hk, hv = heads * keys, heads * values
    blocks = seqs // BLOCK
    hp = nsrow.shape[0]
    up, down, side = {"kv": z + 1}, {"kv": z - 1}, {"tp": 1 - c}

    loads, spans, at = [], [], 0
    for i, src in enumerate((wq_hbm, wk_hbm, wv_hbm, wo_hbm, wi_hbm, wf_hbm)):
        size = src.shape[0]
        spans.append(slice(at, at + size))
        loads.append(
            pltpu.make_async_copy(src, weights.at[pl.ds(at, size)], load_sem.at[i])
        )
        at += size

    def mem_load(b):
        part = pl.ds(b * BLOCK, BLOCK)
        return pltpu.make_async_copy(mem_hbm.at[part], mem.at[part], mem_sem.at[b])

    def own_load(d):
        col = pl.multiple_of((2 * d + c) * width, width)
        return pltpu.make_async_copy(
            out_hbm.at[:, pl.ds(col, width)], w_ref.at[d, pl.ds(0, hv)], wload_sem.at[d]
        )

    def out_piece(d):
        col = pl.multiple_of((2 * d + 1 - c) * width, width)
        return pltpu.make_async_remote_copy(
            src_ref=out_hbm.at[:, pl.ds(col, width)], dst_ref=w_ref.at[d, pl.ds(hv, hv)],
            send_sem=wsend_sem.at[d], recv_sem=wrecv_sem.at[d],
            device_id=side, device_id_type=MESH,
        )

    def hop(slot, p, way, target):
        part = pl.ds(p * piece, piece)
        return pltpu.make_async_remote_copy(
            src_ref=xg.at[slot, 0, part], dst_ref=xg.at[slot, 0, part],
            send_sem=send0.at[way, slot, p], recv_sem=recv0.at[slot, p],
            device_id=target, device_id_type=MESH,
        )

    mine = 2 * z + c

    def direct(target):
        return pltpu.make_async_remote_copy(
            src_ref=xg.at[mine, 1], dst_ref=xg.at[mine, 1],
            send_sem=send1.at[target], recv_sem=recv1.at[mine],
            device_id={"kv": target}, device_id_type=MESH,
        )

    def across(slot):
        return pltpu.make_async_remote_copy(
            src_ref=xg.at[slot, 1], dst_ref=xg.at[slot, 1],
            send_sem=side1.at[slot], recv_sem=recv1.at[slot],
            device_id=side, device_id_type=MESH,
        )

    def arrived(slot):
        return pltpu.make_async_remote_copy(
            src_ref=xg.at[slot, 1], dst_ref=xg.at[slot, 1],
            send_sem=side1.at[slot], recv_sem=recv1.at[slot],
            device_id=side, device_id_type=MESH,
        )

    for load in loads:
        load.start()
    flat = x_ref[...].reshape(rows, width)
    for half in range(HALVES):
        xg[mine, half] = flat[half * lanes : (half + 1) * lanes]
    enter(n, z, c)

    for p in range(PIECES):
        @pl.when(z < n - 1)
        def _():
            hop(mine, p, 0, up).start()

        @pl.when(z > 0)
        def _():
            hop(mine, p, 1, down).start()

    for p in range(PIECES):
        hop(mine, p, 2, side).start()
    across(mine).start()

    @pl.when(z == 0)
    def _():
        direct(z + 1).start()

    @pl.when(z == n - 1)
    def _():
        direct(z - 1).start()

    for b in range(blocks):
        mem_load(b).start()
    for d in range(n):
        own_load(d).start()
        out_piece(d).start()

    acc[...] = jnp.zeros_like(acc)
    squares[...] = jnp.zeros_like(squares)

    expand = (iota((seqs, rows), 0) == iota((seqs, rows), 1) // span).astype(F32)
    lane_pos = iota((span, rows), 1) % span == iota((span, rows), 0)
    dropped = iota((span, seqs), 0) >= acc_ref[...]
    stack, decays, tops = [], [], []
    for h in range(heads):
        stab = stab_ref[h : h + 1, :]
        f = jnp.where(dropped, 0.0, pf_ref[:, h, :])
        i = jnp.where(dropped, FAR_NEGATIVE, pi_ref[:, h, :])
        run = []
        for j in range(span):
            run.append(f[j : j + 1] + run[-1] if run else f[0:1])
        e = run[-1]
        u = e - jnp.concatenate(run, axis=0) + i
        ns = jnp.maximum(e + stab, jnp.max(u, axis=0, keepdims=True))
        ns_out[h : h + 1, :] = ns
        tops.append(ns)
        decays.append(jnp.exp(e + stab - ns))
        stack += [jnp.exp(u - ns), jnp.zeros((8 - span, seqs), F32)]
    tops.append(jnp.zeros((hp - heads, seqs), F32))
    wide = nn(jnp.concatenate(stack + tops, axis=0), expand, HIGHEST)
    nsrow[...] = wide[8 * heads :]
    decays = jnp.concatenate(decays + [jnp.zeros((hp - heads, seqs), F32)], axis=0).T
    old_keys = pk_ref[...].astype(F32).reshape(rows, heads, keys)
    old_values = pv_ref[...].astype(F32).reshape(rows, heads, values)
    odd = (iota((rows, keys), 0) // span) % 2
    spread = iota((seqs, rows), 0) == iota((seqs, rows), 1) // span
    for h in range(heads):
        share_row = jnp.sum(
            jnp.where(lane_pos, wide[8 * h : 8 * h + span], 0.0), axis=0, keepdims=True
        )
        old = old_keys[:, h, :].astype(BF16)
        kps[h] = jnp.concatenate(
            [jnp.where(odd == p, old, jnp.zeros_like(old)) for p in range(2)], axis=1
        )
        part = slice(h * values, (h + 1) * values)
        vts[part, :] = (old_values[:, h, :].T * share_row).astype(BF16)
        full = jnp.broadcast_to(decays[:, h : h + 1], (seqs, keys))
        dfull[h] = full
        after = full * nrm_ref[:, h, :] + nn(jnp.where(spread, share_row, 0.0).astype(BF16), old)
        nn_out[:, h, :] = after
        nrmb[h] = after.astype(BF16)

    def remember(b):
        mem_load(b).wait()
        first = b * BLOCK
        start = pl.multiple_of((first * span) // 128 * 128, 128)
        half = pl.ds(start, 128)
        pair = ((iota((values, 128), 1) + start) // span - first) // 2
        for h in range(heads):
            shared = vts[h * values : (h + 1) * values, half]
            zero = jnp.zeros_like(shared)
            left = jnp.concatenate(
                [jnp.where(pair == s, shared, zero) for s in range(BLOCK // 2)], axis=0
            )
            update = nn(left, kps[h, half, :])
            pairs = []
            for s in range(BLOCK // 2):
                old = jnp.concatenate([mem[first + 2 * s, h], mem[first + 2 * s + 1, h]], axis=1)
                decay = jnp.concatenate(
                    [dfull[h, pl.ds(first + 2 * s + p, 1), :] for p in range(2)], axis=1
                )
                pairs.append((decay * old + update[s * values : (s + 1) * values]).astype(BF16))
            for s in range(BLOCK // 4):
                packed[h, b * (BLOCK // 4) + s] = jnp.concatenate(pairs[2 * s : 2 * s + 2], axis=1)

    def process(owner, half):
        cols = pl.ds(pl.multiple_of(owner * 2 * width, 2 * width), 2 * width)
        x = jnp.concatenate([xg[2 * owner, half], xg[2 * owner + 1, half]], axis=1).astype(F32)
        square = x * x
        total = squares[half]
        for i in range(2 * width // 128):
            total = total + square[:, i * 128 : (i + 1) * 128]
        squares[half] = total
        acc[half] += nt(weights[:, cols], (x * gain_ref[:, cols]).astype(BF16))

    def process_first(owner):
        for p in range(PIECES):
            hop(2 * owner + 1 - c, p, 2, side).wait_recv()
        process(owner, 0)

    def process_second(owner):
        arrived(2 * owner + 1 - c).wait_recv()
        process(owner, 1)

    for load in loads:
        load.wait()
    per = -(-(blocks // HALVES) // (n - 1))

    def gather_first(k, carry):
        for p in range(PIECES):
            @pl.when(z - k >= 0)
            def _():
                slot = 2 * (z - k) + c
                hop(slot, p, 0, up).wait_recv()

                @pl.when(z < n - 1)
                def _():
                    hop(slot, p, 0, up).start()

                hop(slot, p, 2, side).start()

            @pl.when(z + k <= n - 1)
            def _():
                slot = 2 * (z + k) + c
                hop(slot, p, 1, down).wait_recv()

                @pl.when(z > 0)
                def _():
                    hop(slot, p, 1, down).start()

                hop(slot, p, 2, side).start()

        @pl.when((k == z) & (z < n - 1))
        def _():
            direct(z + 1).start()

        @pl.when((k == n - 1 - z) & (z > 0))
        def _():
            direct(z - 1).start()

        @pl.when(z - (k - 1) >= 0)
        def _():
            process_first(z - (k - 1))

        @pl.when((k > 1) & (z + k - 1 <= n - 1))
        def _():
            process_first(z + k - 1)

        for j in range(per):
            b = (k - 1) * per + j

            @pl.when(b < blocks // HALVES)
            def _():
                remember(b)

        return carry

    lax.fori_loop(1, n, gather_first, 0)

    def far(j, carry):
        dist = n - 1 - j

        @pl.when(z + dist <= n - 1)
        def _():
            direct(z + dist).start()

        @pl.when(z - dist >= 0)
        def _():
            direct(z - dist).start()

        return carry

    lax.fori_loop(0, n - 2, far, 0)

    @pl.when(z == n - 1)
    def _():
        process_first(z - (n - 1))

    @pl.when(z == 0)
    def _():
        process_first(z + n - 1)

    place = iota((hp, lanes), 1) % span
    local_gain = hgain_ref[:, :values]
    for i in range(1, hgain_ref.shape[1] // values):
        local_gain = jnp.where(c == i, hgain_ref[:, i * values : (i + 1) * values], local_gain)
    gains = local_gain[:heads]
    for i in range(1, hgain_ref.shape[0] // heads):
        gains = jnp.where(z == i, local_gain[i * heads : (i + 1) * heads], gains)
    columns = jnp.concatenate([gains, jnp.zeros((hp - heads, values), F32)], axis=0).T

    def recur(half):
        part_of = pl.ds(half * lanes, lanes)
        summed = nt(jnp.ones((8, 128), F32), squares[half], HIGHEST)
        inv = lax.rsqrt(summed[0:1] / depth + EPS)
        q, k, v, og, gi, gf = [acc[half, part, :] * inv for part in spans]
        q = (q.astype(BF16).astype(F32) * keys ** (-0.5)).astype(BF16)
        k_rows = k.T.astype(BF16)
        v = v.astype(BF16)
        k_out[part_of, :] = k_rows
        v_out[part_of, :] = v.astype(F32).T.astype(BF16)
        all_heads = gf.shape[0]
        diagonal = iota((all_heads, all_heads), 0) == iota((all_heads, all_heads), 1)
        shift = nn(jnp.where(diagonal, bias_ref[...], 0.0), jnp.ones(gf.shape, F32), HIGHEST)
        raw = gf + shift
        gf = jnp.minimum(raw, 0.0) - jnp.log1p(jnp.exp(-jnp.abs(raw)))
        chosen = []
        for total in (gi, gf):
            out = total[:heads]
            for i in range(1, n):
                out = jnp.where(z == i, total[i * heads : (i + 1) * heads], out)
            chosen.append(jnp.concatenate([out, jnp.zeros((hp - heads, lanes), F32)], axis=0))
        inflow, run = chosen
        gates[0, :, part_of] = inflow
        gates[1, :, part_of] = run
        step = 1
        while step < span:
            run = run + jnp.where(place >= step, pltpu.roll(run, step, 1), 0.0)
            step *= 2
        deltas = [inflow]
        for i in range(1, span):
            spread_i = run - pltpu.roll(run, i, 1) + pltpu.roll(inflow, i, 1)
            deltas.append(jnp.where(place >= i, spread_i, FAR_NEGATIVE))
        carried = run + nsrow[:, part_of]
        top = carried
        for d in deltas:
            top = jnp.maximum(top, d)
        scale = jnp.exp(carried - top)
        floor = jnp.exp(-top)
        ws = [jnp.exp(d - top) for d in deltas]
        placed = []
        for u in range(span):
            w = jnp.zeros_like(top)
            for i in range(span):
                w = jnp.where(place - u == i, ws[i], w)
            placed.append(w)
        same = iota((lanes, lanes), 0) // span == iota((lanes, lanes), 1) // span
        owner = iota(q.shape, 0) // keys
        count = lanes // span
        here = iota((count, lanes), 0) == iota((count, lanes), 1) // span
        quarter = (iota((keys, lanes), 1) // span) % 4
        quad = iota((values, lanes), 1) // span // 4
        for h in range(heads):
            part = slice(h * values, (h + 1) * values)
            query = q[h * keys : (h + 1) * keys]
            none = jnp.zeros_like(query)
            four = jnp.concatenate([jnp.where(quarter == p, query, none) for p in range(4)], axis=0)
            table = packed[h, half * (count // 4) : (half + 1) * (count // 4)]
            read = nn(table.reshape(count // 4 * values, 4 * keys), four)
            recalled = read[:values]
            for s in range(1, count // 4):
                recalled = jnp.where(quad == s, read[s * values : (s + 1) * values], recalled)
            only = jnp.where(owner == h, q, jnp.zeros_like(q))
            w = jnp.concatenate([placed[u][h : h + 1] for u in range(span)] * (8 // span), axis=0)
            w = jnp.broadcast_to(w[None], (lanes // 8, 8, lanes)).reshape(lanes, lanes)
            w = jnp.where(same, w * nn(k_rows, only), 0.0)
            nq = nn(nrmb[h, half * count : (half + 1) * count], query)
            nq = jnp.sum(jnp.where(here, nq, 0.0), axis=0, keepdims=True)
            carry = scale[h : h + 1]
            over = nn(v[part], w.astype(BF16)) + carry * recalled
            under = jnp.sum(w, axis=0, keepdims=True) + carry * nq
            cell = over / jnp.maximum(jnp.abs(under), floor[h : h + 1])
            sq_own[half, h : h + 1, :] = jnp.sum(cell * cell, axis=0, keepdims=True)
            g = jax.nn.sigmoid(og[part]) * cell * columns[:, h : h + 1]
            g_own[half, part, :] = g.astype(BF16)

    def swaps(half):
        return [
            pltpu.make_async_remote_copy(
                src_ref=src.at[half], dst_ref=dst.at[half],
                send_sem=ex_send.at[half, i], recv_sem=ex_recv.at[half, i],
                device_id=side, device_id_type=MESH,
            )
            for i, (src, dst) in enumerate(((g_own, g_in), (sq_own, sq_in)))
        ]

    def join(half):
        for swap in swaps(half):
            swap.wait_recv()
        inv = lax.rsqrt((sq_own[half] + sq_in[half]) / full_values + EPS)
        for i, src in enumerate((g_own, g_in)):
            scaled = jnp.concatenate(
                [
                    src[half, h * values : (h + 1) * values, :].astype(F32) * inv[h : h + 1, :]
                    for h in range(heads)
                ],
                axis=0,
            )
            both[half * lanes : (half + 1) * lanes, i * hv : (i + 1) * hv] = scaled.T.astype(BF16)

    def partial(d, r):
        return nn(both[r * piece : (r + 1) * piece], w_ref[d])

    def upward(d, r):
        return pltpu.make_async_remote_copy(
            src_ref=to_high.at[d, r], dst_ref=from_low.at[d, r],
            send_sem=up_send.at[d, r], recv_sem=up_recv.at[d, r],
            device_id=up, device_id_type=MESH,
        )

    def downward(d, r):
        return pltpu.make_async_remote_copy(
            src_ref=to_low.at[d, r], dst_ref=from_high.at[d, r],
            send_sem=down_send.at[d, r], recv_sem=down_recv.at[d, r],
            device_id=down, device_id_type=MESH,
        )

    def send_first(half):
        def body(i, carry):
            for p in range(PIECES):
                r = half * PIECES + p

                @pl.when(z == 0)
                def _():
                    to_high[n - 1 - i, r] = partial(n - 1 - i, r).astype(BF16)
                    upward(n - 1 - i, r).start()

                @pl.when(z == n - 1)
                def _():
                    to_low[i, r] = partial(i, r).astype(BF16)
                    downward(i, r).start()

            return carry

        lax.fori_loop(0, n - 1, body, 0)

    def send_next(half):
        def body(i, carry):
            high = n - 1 - i + z
            low = i - (n - 1 - z)
            for p in range(PIECES):
                r = half * PIECES + p

                @pl.when((z > 0) & (high > z) & (high <= n - 1))
                def _():
                    term = partial(high, r)
                    upward(high, r).wait_recv()
                    to_high[high, r] = (term + from_low[high, r].astype(F32)).astype(BF16)
                    upward(high, r).start()

                @pl.when((z < n - 1) & (low < z) & (low >= 0))
                def _():
                    term = partial(low, r)
                    downward(low, r).wait_recv()
                    to_low[low, r] = (term + from_high[low, r].astype(F32)).astype(BF16)
                    downward(low, r).start()

            return carry

        lax.fori_loop(0, 2 * n - 2, body, 0)

    recur(0)
    for swap in swaps(0):
        swap.start()

    def rest(b, carry):
        remember(b)
        return carry

    lax.fori_loop(blocks // HALVES, blocks, rest, 0)
    for d in range(n):
        own_load(d).wait()
        out_piece(d).wait_recv()
    join(0)
    send_first(0)

    def gather_second(k, carry):
        @pl.when(z - k >= 0)
        def _():
            slot = 2 * (z - k) + c
            arrived(slot).wait_recv()
            across(slot).start()

        @pl.when(z + k <= n - 1)
        def _():
            slot = 2 * (z + k) + c
            arrived(slot).wait_recv()
            across(slot).start()

        @pl.when(z - (k - 1) >= 0)
        def _():
            process_second(z - (k - 1))

        @pl.when((k > 1) & (z + k - 1 <= n - 1))
        def _():
            process_second(z + k - 1)

        return carry

    lax.fori_loop(1, n, gather_second, 0)

    @pl.when(z == n - 1)
    def _():
        process_second(z - (n - 1))

    @pl.when(z == 0)
    def _():
        process_second(z + n - 1)

    recur(1)
    for swap in swaps(1):
        swap.start()
    join(1)
    send_first(1)
    send_next(0)
    send_next(1)

    for r in range(HALVES * PIECES):
        total_ref[r] = partial(z, r)
    single = [
        jnp.where(lane_pos, gates[i, h : h + 1, :], 0.0) for h in range(heads) for i in range(2)
    ]
    compact = nt(jnp.concatenate(single, axis=0), expand, HIGHEST)
    for h in range(heads):
        ni_out[:, h, :] = compact[2 * h * span : (2 * h + 1) * span]
        nf_out[:, h, :] = compact[(2 * h + 1) * span : (2 * h + 2) * span]
    for r in range(HALVES * PIECES):
        @pl.when(z > 0)
        def _():
            upward(z, r).wait_recv()
            total_ref[r] += from_low[z, r].astype(F32)

        @pl.when(z < n - 1)
        def _():
            downward(z, r).wait_recv()
            total_ref[r] += from_high[z, r].astype(F32)

        y_out[r * piece : (r + 1) * piece, :] = total_ref[r].astype(BF16)

    def drain(i, carry):
        slot = 2 * i + c
        for p in range(PIECES):
            @pl.when((i <= z) & (z < n - 1))
            def _():
                hop(slot, p, 0, up).wait_send()

            @pl.when((i >= z) & (z > 0))
            def _():
                hop(slot, p, 1, down).wait_send()

            hop(slot, p, 2, side).wait_send()

        across(slot).wait_send()
        out_piece(i).wait_send()

        @pl.when(i != z)
        def _():
            direct(i).wait_send()

        for r in range(HALVES * PIECES):
            @pl.when(i > z)
            def _():
                upward(i, r).wait_send()

            @pl.when(i < z)
            def _():
                downward(i, r).wait_send()

        return carry

    lax.fori_loop(0, n, drain, 0)
    for half in range(HALVES):
        for swap in swaps(half):
            swap.wait_send()


def finish_kernel(
    mem_ref, vts, kps, dfull, y_ref, k_ref, v_ref, nn_ref, ns_ref, ni_ref, nf_ref,
    nm_out, y_out, k_out, v_out, nn_out, ns_out, ni_out, nf_out,
    k_tmp, v_tmp,
):
    step = pl.program_id(0)
    block, heads, values, keys = mem_ref.shape
    _, span, width = y_out.shape
    lanes = 128

    @pl.when(step == 0)
    def _():
        nn_out[...] = nn_ref[...]
        ns_out[...] = ns_ref[...]
        ni_out[...] = ni_ref[...]
        nf_out[...] = nf_ref[...]

    y_out[...] = y_ref[...].astype(F32).reshape(block, span, width).astype(BF16)
    for src, tmp, out, size in ((k_ref, k_tmp, k_out, keys), (v_ref, v_tmp, v_out, values)):
        full = src[...].astype(F32)
        for h in range(heads):
            tmp[:, h, :] = full[:, h * size : (h + 1) * size]
        out[...] = tmp[...].reshape(block, span, heads, size).astype(BF16)

    first = step * block
    start = pl.multiple_of((first * span) // lanes * lanes, lanes)
    half = pl.ds(start, lanes)
    pair = ((iota((values, lanes), 1) + start) // span - first) // 2
    for h in range(heads):
        shared = vts[h * values : (h + 1) * values, half]
        zero = jnp.zeros_like(shared)
        left = jnp.concatenate(
            [jnp.where(pair == s, shared, zero) for s in range(block // 2)], axis=0
        )
        update = nn(left, kps[h, half, :])
        for s in range(block):
            at = s // 2 * values
            nm_out[s, h] = (
                dfull[h, pl.ds(first + s, 1), :] * mem_ref[s, h]
                + update[at : at + values, s % 2 * keys : (s % 2 + 1) * keys]
            )


def shards(
    n, tokens, norm_gain, w_query, w_key, w_value, w_outgate, w_input, w_forget, forget_bias,
    head_gain, w_out, memory, normalizer, stabilizer, prev_keys, prev_values, prev_input,
    prev_forget, accepted,
):
    seqs, span, width = tokens.shape
    depth, heads, keys = w_query.shape
    values = w_value.shape[2]
    rows = seqs * span
    hk, hv = heads * keys, heads * values
    all_heads = w_input.shape[1]
    sds = jax.ShapeDtypeStruct
    vm = pl.BlockSpec(memory_space=pltpu.VMEM)
    hbm = pl.BlockSpec(memory_space=pl.ANY)
    flip = lambda w: w.transpose(1, 2, 0).reshape(-1, depth)

    lanes = rows // HALVES
    piece = lanes // PIECES
    parts = HALVES * PIECES
    blocks = seqs // BLOCK
    hp = -(-heads // 8) * 8
    channels = 2 * hk + 2 * hv + 2 * all_heads
    dma = lambda *shape: pltpu.SemaphoreType.DMA(shape)
    y, k, v, vts, kps, dfull, new_n, ns, ni, nf = pl.pallas_call(
        functools.partial(fused_kernel, n, keys, head_gain.shape[1]),
        out_shape=[
            sds((rows, width), BF16), sds((rows, hk), BF16), sds((rows, hv), BF16),
            sds((hv, rows), BF16), sds((heads, rows, 2 * keys), BF16), sds((heads, seqs, keys), F32),
            sds(normalizer.shape, F32), sds((heads, seqs), F32),
            sds((span, heads, seqs), F32), sds((span, heads, seqs), F32),
        ],
        in_specs=[vm] * 11 + [hbm] * 8,
        out_specs=[vm] * 10,
        scratch_shapes=[
            pltpu.VMEM((2 * n, HALVES, lanes, width), BF16),
            pltpu.VMEM((channels, depth), BF16),
            pltpu.VMEM((HALVES, channels, lanes), F32),
            pltpu.VMEM((HALVES, lanes, 128), F32),
            pltpu.VMEM(memory.shape, F32),
            pltpu.VMEM((heads, seqs // 4, values, 4 * keys), BF16),
            pltpu.VMEM((heads, seqs, keys), BF16),
            pltpu.VMEM((2, hp, rows), F32),
            pltpu.VMEM((hp, rows), F32),
            pltpu.VMEM((HALVES, hv, lanes), BF16),
            pltpu.VMEM((HALVES, heads, lanes), F32),
            pltpu.VMEM((HALVES, hv, lanes), BF16),
            pltpu.VMEM((HALVES, heads, lanes), F32),
            pltpu.VMEM((rows, 2 * hv), BF16),
            pltpu.VMEM((n, 2 * hv, width), BF16),
        ]
        + [pltpu.VMEM((n, parts, piece, width), BF16)] * 4
        + [
            pltpu.VMEM((parts, piece, width), F32),
            dma(6), dma(blocks), dma(n), dma(n), dma(n),
            dma(3, 2 * n, PIECES), dma(2 * n, PIECES), dma(n), dma(2 * n), dma(2 * n),
            dma(HALVES, 2), dma(HALVES, 2),
        ]
        + [dma(n, parts)] * 4,
        compiler_params=pltpu.CompilerParams(
            collective_id=0, has_side_effects=True, vmem_limit_bytes=VMEM_LIMIT
        ),
        name="fused",
    )(
        tokens, norm_gain.reshape(1, depth), forget_bias.reshape(1, all_heads),
        prev_keys, prev_values, prev_input.transpose(1, 2, 0), prev_forget.transpose(1, 2, 0),
        accepted.reshape(1, seqs), stabilizer.T, normalizer, head_gain,
        flip(w_query), flip(w_key), flip(w_value), flip(w_outgate),
        w_input.T, w_forget.T, memory, w_out.reshape(hv, -1),
    )

    whole = lambda *shape: pl.BlockSpec(shape, lambda i: (0,) * len(shape))
    strip = lambda size: pl.BlockSpec((BLOCK * span, size), lambda i: (i, 0))
    tile = pl.BlockSpec((BLOCK, heads, values, keys), lambda i: (i, 0, 0, 0))
    fresh = lambda size: pl.BlockSpec((BLOCK, span, heads, size), lambda i: (i, 0, 0, 0))
    new_memory, y, k, v, new_n, ns, ni, nf = pl.pallas_call(
        finish_kernel,
        grid=(blocks,),
        out_shape=[
            sds(memory.shape, F32), sds(tokens.shape, BF16), sds((seqs, span, heads, keys), BF16),
            sds((seqs, span, heads, values), BF16), sds(normalizer.shape, F32),
            sds((heads, seqs), F32), sds((span, heads, seqs), F32), sds((span, heads, seqs), F32),
        ],
        in_specs=[
            tile, whole(hv, rows), whole(heads, rows, 2 * keys), whole(heads, seqs, keys),
            strip(width), strip(hk), strip(hv), whole(seqs, heads, keys), whole(heads, seqs),
            whole(span, heads, seqs), whole(span, heads, seqs),
        ],
        out_specs=[
            tile, pl.BlockSpec((BLOCK, span, width), lambda i: (i, 0, 0)), fresh(keys), fresh(values),
            whole(seqs, heads, keys), whole(heads, seqs), whole(span, heads, seqs),
            whole(span, heads, seqs),
        ],
        scratch_shapes=[
            pltpu.VMEM((BLOCK * span, heads, keys), F32),
            pltpu.VMEM((BLOCK * span, heads, values), F32),
        ],
        compiler_params=pltpu.CompilerParams(vmem_limit_bytes=VMEM_LIMIT),
        name="finish",
    )(memory, vts, kps, dfull, y, k, v, new_n, ns, ni, nf)

    return y, new_memory, new_n, ns.T, k, v, ni.transpose(2, 0, 1), nf.transpose(2, 0, 1)


def solution(mesh):
    return jax.shard_map(
        functools.partial(shards, mesh.shape["kv"]),
        mesh=mesh,
        in_specs=(
            P(("grp", "dp"), None, ("kv", "tp")),
            P(),
            P(None, "kv", None),
            P(None, "kv", None),
            P(None, "kv", "tp"),
            P(None, "kv", "tp"),
            P(),
            P(),
            P(),
            P(),
            P("kv", "tp", None),
            P(("grp", "dp"), "kv", "tp", None),
            P(("grp", "dp"), "kv", None),
            P(("grp", "dp"), "kv"),
            P(("grp", "dp"), None, "kv", None),
            P(("grp", "dp"), None, "kv", "tp"),
            P(("grp", "dp"), None, "kv"),
            P(("grp", "dp"), None, "kv"),
            P(("grp", "dp")),
        ),
        out_specs=(
            P(("grp", "dp"), None, ("kv", "tp")),
            P(("grp", "dp"), "kv", "tp", None),
            P(("grp", "dp"), "kv", None),
            P(("grp", "dp"), "kv"),
            P(("grp", "dp"), None, "kv", None),
            P(("grp", "dp"), None, "kv", "tp"),
            P(("grp", "dp"), None, "kv"),
            P(("grp", "dp"), None, "kv"),
        ),
        check_vma=False,
    )
```

time: 67.8 us -> 59.1 us (0.87)
  Pallas kernels: 63.2 us -> 58.1 us
  local copies, waits for them, and re-layouts: 3.59 us -> 0 us
    pallas_call x3 -> x2, Pallas kernels: 63.2 us -> 58.1 us  [the longest x1 47.3 us: shards(): pl.pallas_call(functools.partial(fused_kernel, n, keys, head_gain.shape[1...]
    unnamed x5 -> x0, local copies, waits for them, and re-layouts: 1.75 us -> none
    reshape x2 -> x0, local copies, waits for them, and re-layouts: 1.74 us -> none  [the longest x1 0.87 us: shards(): k.reshape(seqs, span, heads, keys)]
where the time goes in v1:
time: 59.1 us; the launch traced here: 58.8 us
  Pallas kernels  58.1 us (98%)
  between operations  0.65 us (1%)
    pallas_call x1, Pallas kernels, shards(): pl.pallas_call(functools.partial(fused_kernel, n, keys, head_gain.shape[1...  47.3 us
    pallas_call x1, Pallas kernels, shards(): pl.pallas_call(finish_kernel, grid=(blocks,), out_shape=[sds(memory.shape...  10.8 us

profile of v1, /device:TPU:0, one launch (start us, length us, event | category | flops | bytes accessed | tf_op | source)
XLA Modules:
  0.0 58.8 jit_solution(8714200820056115569)
XLA Ops:
  0.6 47.3 %fused.1 = (bf16[256,512]{1,0:T(8,128)(2,1)}, bf16[256,256]{1,0:T(8,128)(2,1)}, bf16[256,256]{1,0:T(8,128)(2,1)}, bf16[256,256]{1,0:T(8,128)(2,1)}, bf16[4,256,1...) custom-call(bf16[64,4,512]{2,1,0:T(4,128)(2,1)} %x_ref.1, ...), custom_call_target="tpu_custom_call" | custom-call | tf_op jit(solution)/shard_map/fused/pallas_call | solution.py:684
  48.0 10.8 %finish.1 = (f32[64,4,64,64]{3,2,1,0:T(8,128)}, bf16[64,4,512]{2,1,0:T(4,128)(2,1)}, bf16[64,4,4,64]{3,2,1,0:T(4,128)(2,1)}, bf16[64,4,4,64]{3,2,1,0:T(4,128)(2,...) custom-call(f32[64,4,64,64]{3,2,1,0:T(8,128)} %mem_ref.1, ...), custom_call_target="tpu_custom_call" | custom-call | tf_op jit(solution)/shard_map/finish/pallas_call | solution.py:735

commit v2 on v1

v2 whole, which is shorter than its diff:
```python
import functools
import jax
import jax.numpy as jnp
from jax import lax
from jax.sharding import PartitionSpec as P
from jax.experimental import pallas as pl
from jax.experimental.pallas import tpu as pltpu

EPS = 1e-06
FAR_NEGATIVE = -1e30
HIGHEST = lax.Precision.HIGHEST
MESH = pl.DeviceIdType.MESH
F32 = jnp.float32
BF16 = jnp.bfloat16
FUSED_LIMIT = 40 << 20
FINISH_LIMIT = 8 << 20
CHUNKS = (2, 2)
PIECES = 2
PIECE = 32
BLOCK = 8


def nn(a, b, precision=None):
    return lax.dot_general(
        a, b, (((1,), (0,)), ((), ())), precision=precision, preferred_element_type=F32
    )


def nt(a, b, precision=None):
    return lax.dot_general(
        a, b, (((1,), (1,)), ((), ())), precision=precision, preferred_element_type=F32
    )


def iota(shape, d):
    return lax.broadcasted_iota(jnp.int32, shape, d)


def enter(n, z, c):
    barrier = pltpu.get_barrier_semaphore()
    pl.semaphore_signal(barrier, inc=1, device_id={"tp": 1 - c}, device_id_type=MESH)

    @pl.when(z > 0)
    def _():
        pl.semaphore_signal(barrier, inc=1, device_id={"kv": z - 1}, device_id_type=MESH)

    @pl.when(z < n - 1)
    def _():
        pl.semaphore_signal(barrier, inc=1, device_id={"kv": z + 1}, device_id_type=MESH)

    peers = 1 + (z > 0).astype(jnp.int32) + (z < n - 1).astype(jnp.int32)
    pl.semaphore_wait(barrier, peers)


def fused_kernel(
    n, key_size, full_values,
    x_ref, gain_ref, bias_ref, pk_ref, pv_ref, pi_ref, pf_ref, acc_ref, stab_ref, nrm_ref, hgain_ref,
    wq_hbm, wk_hbm, wv_hbm, wo_hbm, wi_hbm, wf_hbm, mem_hbm, out_hbm,
    y_out, k_out, v_out, mem, nn_out, ns_out, ni_out, nf_out,
    xg, weights, acc, squares, vts, kps, dfull, packed, nrmb, gates, nsrow, k_all, v_all, k_tmp, v_tmp, g_own, sq_own, g_in, sq_in, both,
    w_ref, from_low, from_high, to_high, to_low, term_ref, total_ref,
    load_sem, mem_sem, wload_sem, wsend_sem, wrecv_sem,
    send0, recv0, send1, side1, recv1, ex_send, ex_recv, up_send, up_recv, down_send, down_recv,
):
    z = lax.axis_index("kv")
    c = lax.axis_index("tp")
    seqs, span, width = x_ref.shape
    rows = seqs * span
    unit = rows // sum(CHUNKS)
    chunks, start = [], 0
    for size in CHUNKS:
        chunks.append((start * unit, size * unit))
        start += size
    wide_lanes = acc.shape[2]
    piece = chunks[0][1] // PIECES
    depth = gain_ref.shape[1]
    keys = key_size
    heads, values = pv_ref.shape[2:]
    hk, hv = heads * keys, heads * values
    blocks = seqs // BLOCK
    hp = nsrow.shape[0]
    up, down, side = {"kv": z + 1}, {"kv": z - 1}, {"tp": 1 - c}

    loads, spans, at = [], [], 0
    for i, src in enumerate((wq_hbm, wk_hbm, wv_hbm, wo_hbm, wi_hbm, wf_hbm)):
        size = src.shape[0]
        spans.append(slice(at, at + size))
        loads.append(
            pltpu.make_async_copy(src, weights.at[pl.ds(at, size)], load_sem.at[i])
        )
        at += size

    def mem_load(b):
        part = pl.ds(b * BLOCK, BLOCK)
        return pltpu.make_async_copy(mem_hbm.at[part], mem.at[part], mem_sem.at[b])

    def own_load(d):
        col = pl.multiple_of((2 * d + c) * width, width)
        return pltpu.make_async_copy(
            out_hbm.at[:, pl.ds(col, width)], w_ref.at[d, pl.ds(0, hv)], wload_sem.at[d]
        )

    def out_piece(d):
        col = pl.multiple_of((2 * d + 1 - c) * width, width)
        return pltpu.make_async_remote_copy(
            src_ref=out_hbm.at[:, pl.ds(col, width)], dst_ref=w_ref.at[d, pl.ds(hv, hv)],
            send_sem=wsend_sem.at[d], recv_sem=wrecv_sem.at[d],
            device_id=side, device_id_type=MESH,
        )

    def hop(slot, p, way, target):
        part = pl.ds(p * piece, piece)
        return pltpu.make_async_remote_copy(
            src_ref=xg.at[slot, part], dst_ref=xg.at[slot, part],
            send_sem=send0.at[way, slot, p], recv_sem=recv0.at[slot, p],
            device_id=target, device_id_type=MESH,
        )

    mine = 2 * z + c

    def direct(ch, target):
        part = pl.ds(*chunks[ch])
        return pltpu.make_async_remote_copy(
            src_ref=xg.at[mine, part], dst_ref=xg.at[mine, part],
            send_sem=send1.at[ch, target], recv_sem=recv1.at[ch, mine],
            device_id={"kv": target}, device_id_type=MESH,
        )

    def across(ch, slot):
        part = pl.ds(*chunks[ch])
        return pltpu.make_async_remote_copy(
            src_ref=xg.at[slot, part], dst_ref=xg.at[slot, part],
            send_sem=side1.at[ch, slot], recv_sem=recv1.at[ch, slot],
            device_id=side, device_id_type=MESH,
        )

    for load in loads:
        load.start()
    flat = x_ref[...].reshape(rows, width)
    xg[mine] = flat
    enter(n, z, c)

    for p in range(PIECES):
        @pl.when(z < n - 1)
        def _():
            hop(mine, p, 0, up).start()

        @pl.when(z > 0)
        def _():
            hop(mine, p, 1, down).start()

    for p in range(PIECES):
        hop(mine, p, 2, side).start()
    for ch in range(1, len(chunks)):
        across(ch, mine).start()

    @pl.when(z == 0)
    def _():
        direct(1, z + 1).start()

    @pl.when(z == n - 1)
    def _():
        direct(1, z - 1).start()

    for b in range(blocks):
        mem_load(b).start()
    for d in range(n):
        own_load(d).start()
        out_piece(d).start()

    acc[...] = jnp.zeros_like(acc)
    squares[...] = jnp.zeros_like(squares)
    gates[...] = jnp.zeros_like(gates)
    g_own[...] = jnp.zeros_like(g_own)
    sq_own[...] = jnp.zeros_like(sq_own)

    expand = (iota((seqs, rows), 0) == iota((seqs, rows), 1) // span).astype(F32)
    lane_pos = iota((span, rows), 1) % span == iota((span, rows), 0)
    dropped = iota((span, seqs), 0) >= acc_ref[...]
    stack, decays, tops = [], [], []
    for h in range(heads):
        stab = stab_ref[h : h + 1, :]
        f = jnp.where(dropped, 0.0, pf_ref[:, h, :])
        i = jnp.where(dropped, FAR_NEGATIVE, pi_ref[:, h, :])
        run = []
        for j in range(span):
            run.append(f[j : j + 1] + run[-1] if run else f[0:1])
        e = run[-1]
        u = e - jnp.concatenate(run, axis=0) + i
        ns = jnp.maximum(e + stab, jnp.max(u, axis=0, keepdims=True))
        ns_out[h : h + 1, :] = ns
        tops.append(ns)
        decays.append(jnp.exp(e + stab - ns))
        stack += [jnp.exp(u - ns), jnp.zeros((8 - span, seqs), F32)]
    tops.append(jnp.zeros((hp - heads, seqs), F32))
    wide = nn(jnp.concatenate(stack, axis=0), expand, HIGHEST)
    shape = (seqs, len(chunks) * wide_lanes)
    lane = iota(shape, 1)
    padded = jnp.zeros(shape, jnp.bool_)
    for ch, (r0, m) in enumerate(chunks):
        at = lane - ch * wide_lanes
        padded = padded | ((at >= 0) & (at < m) & (iota(shape, 0) == (at + r0) // span))
    padded = padded.astype(F32)
    nsrow[...] = nn(jnp.concatenate(tops, axis=0), padded, HIGHEST)
    decays = jnp.concatenate(decays + [jnp.zeros((hp - heads, seqs), F32)], axis=0).T
    old_keys = pk_ref[...].astype(F32).reshape(rows, heads, keys)
    old_values = pv_ref[...].astype(F32).reshape(rows, heads, values)
    odd = (iota((rows, keys), 0) // span) % 2
    spread = iota((seqs, rows), 0) == iota((seqs, rows), 1) // span
    for h in range(heads):
        share_row = jnp.sum(
            jnp.where(lane_pos, wide[8 * h : 8 * h + span], 0.0), axis=0, keepdims=True
        )
        old = old_keys[:, h, :].astype(BF16)
        kps[h] = jnp.concatenate(
            [jnp.where(odd == p, old, jnp.zeros_like(old)) for p in range(2)], axis=1
        )
        part = slice(h * values, (h + 1) * values)
        vts[part, :] = (old_values[:, h, :].T * share_row).astype(BF16)
        full = jnp.broadcast_to(decays[:, h : h + 1], (seqs, keys))
        dfull[h] = full
        after = full * nrm_ref[:, h, :] + nn(jnp.where(spread, share_row, 0.0).astype(BF16), old)
        nn_out[:, h, :] = after
        nrmb[h] = after.astype(BF16)

    def remember(b):
        mem_load(b).wait()
        first = b * BLOCK
        start = pl.multiple_of((first * span) // 128 * 128, 128)
        half = pl.ds(start, 128)
        pair = ((iota((values, 128), 1) + start) // span - first) // 2
        for h in range(heads):
            shared = vts[h * values : (h + 1) * values, half]
            zero = jnp.zeros_like(shared)
            left = jnp.concatenate(
                [jnp.where(pair == s, shared, zero) for s in range(BLOCK // 2)], axis=0
            )
            update = nn(left, kps[h, half, :])
            pairs = []
            for s in range(BLOCK // 2):
                after = []
                for p in range(2):
                    seq = first + 2 * s + p
                    fresh = update[s * values : (s + 1) * values, p * keys : (p + 1) * keys]
                    after.append(dfull[h, pl.ds(seq, 1), :] * mem[seq, h] + fresh)
                    mem[seq, h] = after[p]
                pairs.append(jnp.concatenate(after, axis=1).astype(BF16))
            for s in range(BLOCK // 4):
                packed[h, b * (BLOCK // 4) + s] = jnp.concatenate(pairs[2 * s : 2 * s + 2], axis=1)

    def process(owner, ch):
        r0, m = chunks[ch]
        cols = pl.ds(pl.multiple_of(owner * 2 * width, 2 * width), 2 * width)
        x = jnp.concatenate(
            [xg[2 * owner + i, pl.ds(r0, m), :] for i in range(2)], axis=1
        ).astype(F32)
        square = x * x
        total = squares[ch, :m]
        for i in range(2 * width // 128):
            total = total + square[:, i * 128 : (i + 1) * 128]
        squares[ch, :m] = total
        acc[ch, :, :m] += nt(weights[:, cols], (x * gain_ref[:, cols]).astype(BF16))

    def process_first(owner):
        for p in range(PIECES):
            hop(2 * owner + 1 - c, p, 2, side).wait_recv()
        process(owner, 0)

    def process_later(owner, ch):
        across(ch, 2 * owner + 1 - c).wait_recv()
        process(owner, ch)

    for load in loads:
        load.wait()
    per = -(-blocks // (n - 1))

    def remember_some(k):
        for j in range(per):
            b = k * per + j

            @pl.when(b < blocks)
            def _():
                remember(b)

    process_first(z)
    remember_some(0)

    def pair(k):
        return ((z + k, z + k <= n - 1), (z - k, z - k >= 0))

    def send_later(k):
        for target, there in pair(k):
            @pl.when(there)
            def _():
                direct(1, target).start()

    def gather_first(k, carry):
        @pl.when(k > 2)
        def _():
            send_later(k - 1)

        for p in range(PIECES):
            @pl.when(z - k >= 0)
            def _():
                slot = 2 * (z - k) + c
                hop(slot, p, 0, up).wait_recv()

                @pl.when(z < n - 1)
                def _():
                    hop(slot, p, 0, up).start()

                hop(slot, p, 2, side).start()

            @pl.when(z + k <= n - 1)
            def _():
                slot = 2 * (z + k) + c
                hop(slot, p, 1, down).wait_recv()

                @pl.when(z > 0)
                def _():
                    hop(slot, p, 1, down).start()

                hop(slot, p, 2, side).start()

        @pl.when((k == z) & (z < n - 1))
        def _():
            direct(1, z + 1).start()

        @pl.when((k == n - 1 - z) & (z > 0))
        def _():
            direct(1, z - 1).start()

        @pl.when(k < n - 1)
        def _():
            remember_some(k)

            for owner, there in pair(k):
                @pl.when(there)
                def _():
                    process_first(owner)

        return carry

    lax.fori_loop(1, n, gather_first, 0)

    if n > 2:
        send_later(n - 1)
    process_later(z, 1)
    for owner, there in pair(n - 1):
        @pl.when(there)
        def _():
            process_first(owner)

    local_gain = hgain_ref[:, :values]
    for i in range(1, hgain_ref.shape[1] // values):
        local_gain = jnp.where(c == i, hgain_ref[:, i * values : (i + 1) * values], local_gain)
    gains = local_gain[:heads]
    for i in range(1, hgain_ref.shape[0] // heads):
        gains = jnp.where(z == i, local_gain[i * heads : (i + 1) * heads], gains)
    columns = jnp.concatenate([gains, jnp.zeros((hp - heads, values), F32)], axis=0).T

    def recur(ch):
        r0, lanes = chunks[ch]
        part_of = pl.ds(r0, lanes)
        padded_part = pl.ds(ch * wide_lanes, lanes)
        place = iota((hp, lanes), 1) % span
        summed = nt(jnp.ones((8, 128), F32), squares[ch, :lanes], HIGHEST)
        inv = lax.rsqrt(summed[0:1] / depth + EPS)
        q, k, v, og, gi, gf = [acc[ch, part, :lanes] * inv for part in spans]
        q = (q.astype(BF16).astype(F32) * keys ** (-0.5)).astype(BF16)
        k_rows = k.T.astype(BF16)
        v = v.astype(BF16)
        k_all[part_of, :] = k_rows
        v_all[part_of, :] = v.astype(F32).T.astype(BF16)
        all_heads = gf.shape[0]
        diagonal = iota((all_heads, all_heads), 0) == iota((all_heads, all_heads), 1)
        shift = nn(jnp.where(diagonal, bias_ref[...], 0.0), jnp.ones(gf.shape, F32), HIGHEST)
        raw = gf + shift
        gf = jnp.minimum(raw, 0.0) - jnp.log1p(jnp.exp(-jnp.abs(raw)))
        chosen = []
        for total in (gi, gf):
            out = total[:heads]
            for i in range(1, n):
                out = jnp.where(z == i, total[i * heads : (i + 1) * heads], out)
            chosen.append(jnp.concatenate([out, jnp.zeros((hp - heads, lanes), F32)], axis=0))
        inflow, run = chosen
        gates[0, :, padded_part] = inflow
        gates[1, :, padded_part] = run
        step = 1
        while step < span:
            run = run + jnp.where(place >= step, pltpu.roll(run, step, 1), 0.0)
            step *= 2
        deltas = [inflow]
        for i in range(1, span):
            spread_i = run - pltpu.roll(run, i, 1) + pltpu.roll(inflow, i, 1)
            deltas.append(jnp.where(place >= i, spread_i, FAR_NEGATIVE))
        carried = run + nsrow[:, padded_part]
        top = carried
        for d in deltas:
            top = jnp.maximum(top, d)
        scale = jnp.exp(carried - top)
        floor = jnp.exp(-top)
        ws = [jnp.exp(d - top) for d in deltas]
        placed = []
        for u in range(span):
            w = jnp.zeros_like(top)
            for i in range(span):
                w = jnp.where(place - u == i, ws[i], w)
            placed.append(w)
        same = iota((lanes, lanes), 0) // span == iota((lanes, lanes), 1) // span
        owner = iota(q.shape, 0) // keys
        count = lanes // span
        here = iota((count, lanes), 0) == iota((count, lanes), 1) // span
        quarter = (iota((keys, lanes), 1) // span) % 4
        quad = iota((values, lanes), 1) // span // 4
        for h in range(heads):
            part = slice(h * values, (h + 1) * values)
            query = q[h * keys : (h + 1) * keys]
            none = jnp.zeros_like(query)
            four = jnp.concatenate([jnp.where(quarter == p, query, none) for p in range(4)], axis=0)
            table = packed[h, r0 // span // 4 : (r0 // span + count) // 4]
            read = nn(table.reshape(count // 4 * values, 4 * keys), four)
            recalled = read[:values]
            for s in range(1, count // 4):
                recalled = jnp.where(quad == s, read[s * values : (s + 1) * values], recalled)
            only = jnp.where(owner == h, q, jnp.zeros_like(q))
            w = jnp.concatenate([placed[u][h : h + 1] for u in range(span)] * (8 // span), axis=0)
            w = jnp.broadcast_to(w[None], (lanes // 8, 8, lanes)).reshape(lanes, lanes)
            w = jnp.where(same, w * nn(k_rows, only), 0.0)
            nq = nn(nrmb[h, r0 // span : r0 // span + count], query)
            nq = jnp.sum(jnp.where(here, nq, 0.0), axis=0, keepdims=True)
            carry = scale[h : h + 1]
            over = nn(v[part], w.astype(BF16)) + carry * recalled
            under = jnp.sum(w, axis=0, keepdims=True) + carry * nq
            cell = over / jnp.maximum(jnp.abs(under), floor[h : h + 1])
            sq_own[ch, h : h + 1, :lanes] = jnp.sum(cell * cell, axis=0, keepdims=True)
            g = jax.nn.sigmoid(og[part]) * cell * columns[:, h : h + 1]
            g_own[ch, part, :lanes] = g.astype(BF16)

    def swaps(ch):
        return [
            pltpu.make_async_remote_copy(
                src_ref=src.at[ch], dst_ref=dst.at[ch],
                send_sem=ex_send.at[ch, i], recv_sem=ex_recv.at[ch, i],
                device_id=side, device_id_type=MESH,
            )
            for i, (src, dst) in enumerate(((g_own, g_in), (sq_own, sq_in)))
        ]

    def join(ch):
        r0, m = chunks[ch]
        for swap in swaps(ch):
            swap.wait_recv()
        inv = lax.rsqrt((sq_own[ch, :, :m] + sq_in[ch, :, :m]) / full_values + EPS)
        for i, src in enumerate((g_own, g_in)):
            scaled = jnp.concatenate(
                [
                    src[ch, h * values : (h + 1) * values, :m].astype(F32) * inv[h : h + 1, :]
                    for h in range(heads)
                ],
                axis=0,
            )
            both[r0 : r0 + m, i * hv : (i + 1) * hv] = scaled.T.astype(BF16)

    def partial(d, ch):
        r0, m = chunks[ch]
        return nn(both[r0 : r0 + m], w_ref[d])

    def upward(d, r):
        return pltpu.make_async_remote_copy(
            src_ref=to_high.at[d, pl.ds(r * PIECE, PIECE)],
            dst_ref=from_low.at[d, pl.ds(r * PIECE, PIECE)],
            send_sem=up_send.at[d, r], recv_sem=up_recv.at[d, r],
            device_id=up, device_id_type=MESH,
        )

    def downward(d, r):
        return pltpu.make_async_remote_copy(
            src_ref=to_low.at[d, pl.ds(r * PIECE, PIECE)],
            dst_ref=from_high.at[d, pl.ds(r * PIECE, PIECE)],
            send_sem=down_send.at[d, r], recv_sem=down_recv.at[d, r],
            device_id=down, device_id_type=MESH,
        )

    def units(ch):
        r0, m = chunks[ch]
        return range(r0 // PIECE, (r0 + m) // PIECE)

    def send_first(ch):
        r0, m = chunks[ch]

        def body(i, carry):
            @pl.when(z == 0)
            def _():
                to_high[n - 1 - i, r0 : r0 + m] = partial(n - 1 - i, ch).astype(BF16)
                for r in units(ch):
                    upward(n - 1 - i, r).start()

            @pl.when(z == n - 1)
            def _():
                to_low[i, r0 : r0 + m] = partial(i, ch).astype(BF16)
                for r in units(ch):
                    downward(i, r).start()

            return carry

        lax.fori_loop(0, n - 1, body, 0)

    def send_next(ch):
        r0, m = chunks[ch]

        def body(i, carry):
            high = n - 1 - i + z
            low = i - (n - 1 - z)
            rising = (z > 0) & (high > z) & (high <= n - 1)
            falling = (z < n - 1) & (low < z) & (low >= 0)

            @pl.when(rising)
            def _():
                term_ref[0, :m] = partial(high, ch)

            @pl.when(falling)
            def _():
                term_ref[1, :m] = partial(low, ch)

            for r in units(ch):
                at = slice(r * PIECE, (r + 1) * PIECE)
                mid = slice(r * PIECE - r0, (r + 1) * PIECE - r0)

                @pl.when(rising)
                def _():
                    upward(high, r).wait_recv()
                    to_high[high, at] = (term_ref[0, mid] + from_low[high, at].astype(F32)).astype(BF16)
                    upward(high, r).start()

                @pl.when(falling)
                def _():
                    downward(low, r).wait_recv()
                    to_low[low, at] = (term_ref[1, mid] + from_high[low, at].astype(F32)).astype(BF16)
                    downward(low, r).start()

            return carry

        lax.fori_loop(0, 2 * n - 2, body, 0)

    def arrive(ch, k):
        for slot, there in ((2 * (z - k) + c, z - k >= 0), (2 * (z + k) + c, z + k <= n - 1)):
            @pl.when(there)
            def _():
                across(ch, slot).wait_recv()
                across(ch, slot).start()

    def work(ch, k):
        for owner, there in ((z - k, z - k >= 0), (z + k, z + k <= n - 1)):
            @pl.when(there)
            def _():
                process_later(owner, ch)

    recur(0)
    for swap in swaps(0):
        swap.start()
    arrive(1, 1)
    for d in range(n):
        own_load(d).wait()
        out_piece(d).wait_recv()
    join(0)
    send_first(0)
    work(1, 1)

    def gather_later(k, carry):
        arrive(1, k)

        @pl.when(k > 2)
        def _():
            work(1, k - 1)

        return carry

    lax.fori_loop(2, n, gather_later, 0)
    work(1, n - 1)
    recur(1)
    for swap in swaps(1):
        swap.start()
    join(1)
    send_first(1)
    send_next(0)
    send_next(1)

    total_ref[...] = nn(both[...], w_ref[z])
    for src, tmp, out, size in ((k_all, k_tmp, k_out, keys), (v_all, v_tmp, v_out, values)):
        full = src[...].astype(F32)
        for h in range(heads):
            tmp[:, h, :] = full[:, h * size : (h + 1) * size]
        out[...] = tmp[...].reshape(seqs, span, heads, size).astype(BF16)
    pos = iota((span, len(chunks) * wide_lanes), 1) % span
    lane_pos = pos == iota((span, len(chunks) * wide_lanes), 0)
    single = [
        jnp.where(lane_pos, gates[i, h : h + 1, :], 0.0) for h in range(heads) for i in range(2)
    ]
    compact = nt(jnp.concatenate(single, axis=0), padded, HIGHEST)
    for h in range(heads):
        ni_out[:, h, :] = compact[2 * h * span : (2 * h + 1) * span]
        nf_out[:, h, :] = compact[(2 * h + 1) * span : (2 * h + 2) * span]
    for r in range(rows // PIECE):
        at = slice(r * PIECE, (r + 1) * PIECE)

        @pl.when(z > 0)
        def _():
            upward(z, r).wait_recv()
            total_ref[at] += from_low[z, at].astype(F32)

        @pl.when(z < n - 1)
        def _():
            downward(z, r).wait_recv()
            total_ref[at] += from_high[z, at].astype(F32)

        count = PIECE // span
        y_out[r * count : (r + 1) * count] = total_ref[at].reshape(count, span, width).astype(BF16)

    def drain(i, carry):
        slot = 2 * i + c
        for p in range(PIECES):
            @pl.when((i <= z) & (z < n - 1))
            def _():
                hop(slot, p, 0, up).wait_send()

            @pl.when((i >= z) & (z > 0))
            def _():
                hop(slot, p, 1, down).wait_send()

            hop(slot, p, 2, side).wait_send()

        out_piece(i).wait_send()
        for ch in range(1, len(chunks)):
            across(ch, slot).wait_send()

            @pl.when(i != z)
            def _():
                direct(ch, i).wait_send()

        for r in range(rows // PIECE):
            @pl.when(i > z)
            def _():
                upward(i, r).wait_send()

            @pl.when(i < z)
            def _():
                downward(i, r).wait_send()

        return carry

    lax.fori_loop(0, n, drain, 0)
    for ch in range(len(chunks)):
        for swap in swaps(ch):
            swap.wait_send()


def finish_kernel(*refs):
    count = (len(refs) - 1) // 2
    sem = refs[-1]
    copies = [
        pltpu.make_async_copy(src, dst, sem.at[i])
        for i, (src, dst) in enumerate(zip(refs[1:count], refs[count + 1 : 2 * count]))
    ]
    memory, new_memory = refs[0], refs[count]
    for b in range(memory.shape[0] // BLOCK):
        part = pl.ds(b * BLOCK, BLOCK)
        copies.append(
            pltpu.make_async_copy(memory.at[part], new_memory.at[part], sem.at[count - 1 + b])
        )
    for copy in copies:
        copy.start()
    for copy in copies:
        copy.wait()


def shards(
    n, tokens, norm_gain, w_query, w_key, w_value, w_outgate, w_input, w_forget, forget_bias,
    head_gain, w_out, memory, normalizer, stabilizer, prev_keys, prev_values, prev_input,
    prev_forget, accepted,
):
    seqs, span, width = tokens.shape
    depth, heads, keys = w_query.shape
    values = w_value.shape[2]
    rows = seqs * span
    hk, hv = heads * keys, heads * values
    all_heads = w_input.shape[1]
    sds = jax.ShapeDtypeStruct
    vm = pl.BlockSpec(memory_space=pltpu.VMEM)
    hbm = pl.BlockSpec(memory_space=pl.ANY)
    flip = lambda w: w.transpose(1, 2, 0).reshape(-1, depth)

    parts = sum(CHUNKS)
    unit = rows // parts
    lanes = -(-unit * max(CHUNKS) // 128) * 128
    count = len(CHUNKS)
    blocks = seqs // BLOCK
    hp = -(-heads // 8) * 8
    channels = 2 * hk + 2 * hv + 2 * all_heads
    dma = lambda *shape: pltpu.SemaphoreType.DMA(shape)
    outs = [
        sds(tokens.shape, BF16), sds((seqs, span, heads, keys), BF16),
        sds((seqs, span, heads, values), BF16), sds(memory.shape, F32),
        sds(normalizer.shape, F32), sds((heads, seqs), F32),
        sds((span, heads, seqs), F32), sds((span, heads, seqs), F32),
    ]
    y, k, v, mem, new_n, ns, ni, nf = pl.pallas_call(
        functools.partial(fused_kernel, n, keys, head_gain.shape[1]),
        out_shape=outs,
        in_specs=[vm] * 11 + [hbm] * 8,
        out_specs=[vm] * 8,
        scratch_shapes=[
            pltpu.VMEM((2 * n, rows, width), BF16),
            pltpu.VMEM((channels, depth), BF16),
            pltpu.VMEM((count, channels, lanes), F32),
            pltpu.VMEM((count, lanes, 128), F32),
            pltpu.VMEM((hv, rows), BF16),
            pltpu.VMEM((heads, rows, 2 * keys), BF16),
            pltpu.VMEM((heads, seqs, keys), F32),
            pltpu.VMEM((heads, seqs // 4, values, 4 * keys), BF16),
            pltpu.VMEM((heads, seqs, keys), BF16),
            pltpu.VMEM((2, hp, count * lanes), F32),
            pltpu.VMEM((hp, count * lanes), F32),
            pltpu.VMEM((rows, hk), BF16),
            pltpu.VMEM((rows, hv), BF16),
            pltpu.VMEM((rows, heads, keys), F32),
            pltpu.VMEM((rows, heads, values), F32),
            pltpu.VMEM((count, hv, lanes), BF16),
            pltpu.VMEM((count, heads, lanes), F32),
            pltpu.VMEM((count, hv, lanes), BF16),
            pltpu.VMEM((count, heads, lanes), F32),
            pltpu.VMEM((rows, 2 * hv), BF16),
            pltpu.VMEM((n, 2 * hv, width), BF16),
        ]
        + [pltpu.VMEM((n, rows, width), BF16)] * 4
        + [
            pltpu.VMEM((2, lanes, width), F32), pltpu.VMEM((rows, width), F32),
            dma(6), dma(blocks), dma(n), dma(n), dma(n),
            dma(3, 2 * n, PIECES), dma(2 * n, PIECES), dma(count, n), dma(count, 2 * n),
            dma(count, 2 * n), dma(count, 2), dma(count, 2),
        ]
        + [dma(n, rows // PIECE)] * 4,
        compiler_params=pltpu.CompilerParams(
            collective_id=0, has_side_effects=True, vmem_limit_bytes=FUSED_LIMIT
        ),
        name="fused",
    )(
        *[
            pltpu.with_memory_space_constraint(a, pltpu.HBM)
            for a in (
                tokens, norm_gain.reshape(1, depth), forget_bias.reshape(1, all_heads),
                prev_keys, prev_values, prev_input.transpose(1, 2, 0),
                prev_forget.transpose(1, 2, 0), accepted.reshape(1, seqs), stabilizer.T,
                normalizer, head_gain,
                flip(w_query), flip(w_key), flip(w_value), flip(w_outgate),
                w_input.T, w_forget.T, memory, w_out.reshape(hv, -1),
            )
        ]
    )

    new_memory, y, k, v, new_n, ns, ni, nf = pl.pallas_call(
        finish_kernel,
        out_shape=[outs[3], *outs[:3], *outs[4:]],
        in_specs=[vm] * 8,
        out_specs=[hbm] * 8,
        scratch_shapes=[dma(7 + blocks)],
        compiler_params=pltpu.CompilerParams(vmem_limit_bytes=FINISH_LIMIT),
        name="finish",
    )(mem, y, k, v, new_n, ns, ni, nf)

    return y, new_memory, new_n, ns.T, k, v, ni.transpose(2, 0, 1), nf.transpose(2, 0, 1)


def solution(mesh):
    return jax.shard_map(
        functools.partial(shards, mesh.shape["kv"]),
        mesh=mesh,
        in_specs=(
            P(("grp", "dp"), None, ("kv", "tp")),
            P(),
            P(None, "kv", None),
            P(None, "kv", None),
            P(None, "kv", "tp"),
            P(None, "kv", "tp"),
            P(),
            P(),
            P(),
            P(),
            P("kv", "tp", None),
            P(("grp", "dp"), "kv", "tp", None),
            P(("grp", "dp"), "kv", None),
            P(("grp", "dp"), "kv"),
            P(("grp", "dp"), None, "kv", None),
            P(("grp", "dp"), None, "kv", "tp"),
            P(("grp", "dp"), None, "kv"),
            P(("grp", "dp"), None, "kv"),
            P(("grp", "dp")),
        ),
        out_specs=(
            P(("grp", "dp"), None, ("kv", "tp")),
            P(("grp", "dp"), "kv", "tp", None),
            P(("grp", "dp"), "kv", None),
            P(("grp", "dp"), "kv"),
            P(("grp", "dp"), None, "kv", None),
            P(("grp", "dp"), None, "kv", "tp"),
            P(("grp", "dp"), None, "kv"),
            P(("grp", "dp"), None, "kv"),
        ),
        check_vma=False,
    )
```

time: 59.1 us -> 50.4 us (0.85)
  Pallas kernels: 58.1 us -> 49.5 us
    pallas_call x1, Pallas kernels: 10.8 us -> 3.75 us  [shards(): pl.pallas_call(finish_kernel, out_shape=[outs[3], *outs[:3], *outs[4:]],...]
    pallas_call x1, Pallas kernels: 47.3 us -> 45.7 us  [shards(): pl.pallas_call(functools.partial(fused_kernel, n, keys, head_gain.shape[1...]
where the time goes in v2:
time: 50.4 us; the launch traced here: 50.3 us
  Pallas kernels  49.5 us (98%)
  between operations  0.81 us (2%)
    pallas_call x1, Pallas kernels, shards(): pl.pallas_call(functools.partial(fused_kernel, n, keys, head_gain.shape[1...  45.7 us
    pallas_call x1, Pallas kernels, shards(): pl.pallas_call(finish_kernel, out_shape=[outs[3], *outs[:3], *outs[4:]],...  3.75 us

profile of v2, /device:TPU:0, one launch (start us, length us, event | category | flops | bytes accessed | tf_op | source)
XLA Modules:
  0.0 50.3 jit_solution(16403043504463512271)
XLA Ops:
  0.6 45.7 %fused.1 = (bf16[64,4,512]{2,1,0:T(4,128)(2,1)S(1)}, bf16[64,4,4,64]{3,2,1,0:T(4,128)(2,1)S(1)}, bf16[64,4,4,64]{3,2,1,0:T(4,128)(2,1)S(1)}, f32[64,4,64,64]{3,2...) custom-call(bf16[64,4,512]{2,1,0:T(4,128)(2,1)} %x_ref.1, ...), custom_call_target="tpu_custom_call" | custom-call | tf_op jit(solution)/shard_map/fused/pallas_call | solution.py:707
  46.4 3.7 %finish.1 = (f32[64,4,64,64]{3,2,1,0:T(8,128)}, bf16[64,4,512]{2,1,0:T(4,128)(2,1)}, bf16[64,4,4,64]{3,2,1,0:T(4,128)(2,1)}, bf16[64,4,4,64]{3,2,1,0:T(4,128)(2,...) custom-call(f32[64,4,64,64]{3,2,1,0:T(8,128)S(1)} %get-tuple-element.24.refs_0_, ...), custom_call_target="tpu_custom_call" | custom-call | tf_op jit(solution)/shard_map/finish/pallas_call | solution.py:761

commit v3 on v2

--- a/solution.py
+++ b/solution.py
@@ -527,18 +527,18 @@
                 at = slice(r * PIECE, (r + 1) * PIECE)
                 mid = slice(r * PIECE - r0, (r + 1) * PIECE - r0)
 
+                @pl.when(falling)
+                def _():
+                    downward(low, r).wait_recv()
+                    to_low[low, at] = (term_ref[1, mid] + from_high[low, at].astype(F32)).astype(BF16)
+                    downward(low, r).start()
+
                 @pl.when(rising)
                 def _():
                     upward(high, r).wait_recv()
                     to_high[high, at] = (term_ref[0, mid] + from_low[high, at].astype(F32)).astype(BF16)
                     upward(high, r).start()
 
-                @pl.when(falling)
-                def _():
-                    downward(low, r).wait_recv()
-                    to_low[low, at] = (term_ref[1, mid] + from_high[low, at].astype(F32)).astype(BF16)
-                    downward(low, r).start()
-
             return carry
 
         lax.fori_loop(0, 2 * n - 2, body, 0)
@@ -555,6 +555,15 @@
             @pl.when(there)
             def _():
                 process_later(owner, ch)
+
+    def settle():
+        for src, tmp, out, size in ((k_all, k_tmp, k_out, keys), (v_all, v_tmp, v_out, values)):
+            full = src[...].astype(F32)
+            for h in range(heads):
+                tmp[:, h, :] = full[:, h * size : (h + 1) * size]
+            out[...] = tmp[...].reshape(seqs, span, heads, size).astype(BF16)
+
+    early = (c == 1) & ((z == 0) | (z == n - 1))
 
     recur(0)
     for swap in swaps(0):
@@ -582,16 +591,20 @@
     for swap in swaps(1):
         swap.start()
     join(1)
+
+    @pl.when(early)
+    def _():
+        settle()
+
     send_first(1)
     send_next(0)
     send_next(1)
 
     total_ref[...] = nn(both[...], w_ref[z])
-    for src, tmp, out, size in ((k_all, k_tmp, k_out, keys), (v_all, v_tmp, v_out, values)):
-        full = src[...].astype(F32)
-        for h in range(heads):
-            tmp[:, h, :] = full[:, h * size : (h + 1) * size]
-        out[...] = tmp[...].reshape(seqs, span, heads, size).astype(BF16)
+    @pl.when(jnp.logical_not(early))
+    def _():
+        settle()
+
     pos = iota((span, len(chunks) * wide_lanes), 1) % span
     lane_pos = pos == iota((span, len(chunks) * wide_lanes), 0)
     single = [
@@ -658,16 +671,15 @@
 def finish_kernel(*refs):
     count = (len(refs) - 1) // 2
     sem = refs[-1]
-    copies = [
-        pltpu.make_async_copy(src, dst, sem.at[i])
-        for i, (src, dst) in enumerate(zip(refs[1:count], refs[count + 1 : 2 * count]))
-    ]
     memory, new_memory = refs[0], refs[count]
+    copies = []
     for b in range(memory.shape[0] // BLOCK):
         part = pl.ds(b * BLOCK, BLOCK)
         copies.append(
             pltpu.make_async_copy(memory.at[part], new_memory.at[part], sem.at[count - 1 + b])
         )
+    for i, (src, dst) in enumerate(zip(refs[1:count], refs[count + 1 : 2 * count])):
+        copies.append(pltpu.make_async_copy(src, dst, sem.at[i]))
     for copy in copies:
         copy.start()
     for copy in copies:

time: 50.4 us -> 49.7 us (0.986)
  Pallas kernels: 49.5 us -> 48.8 us
    pallas_call x1, Pallas kernels: 45.7 us -> 45.1 us  [shards(): pl.pallas_call(functools.partial(fused_kernel, n, keys, head_gain.shape[1...]
where the time goes in v3:
time: 49.7 us; the launch traced here: 49.6 us
  Pallas kernels  48.8 us (98%)
  between operations  0.81 us (2%)
    pallas_call x1, Pallas kernels, shards(): pl.pallas_call(functools.partial(fused_kernel, n, keys, head_gain.shape[1...  45.1 us
    pallas_call x1, Pallas kernels, shards(): pl.pallas_call(finish_kernel, out_shape=[outs[3], *outs[:3], *outs[4:]],...  3.68 us

profile of v3, /device:TPU:0, one launch (start us, length us, event | category | flops | bytes accessed | tf_op | source)
XLA Modules:
  0.0 49.6 jit_solution(16532025229896429600)
XLA Ops:
  0.6 45.1 %fused.1 = (bf16[64,4,512]{2,1,0:T(4,128)(2,1)S(1)}, bf16[64,4,4,64]{3,2,1,0:T(4,128)(2,1)S(1)}, bf16[64,4,4,64]{3,2,1,0:T(4,128)(2,1)S(1)}, f32[64,4,64,64]{3,2...) custom-call(bf16[64,4,512]{2,1,0:T(4,128)(2,1)} %x_ref.1, ...), custom_call_target="tpu_custom_call" | custom-call | tf_op jit(solution)/shard_map/fused/pallas_call | solution.py:719
  45.7 3.7 %finish.1 = (f32[64,4,64,64]{3,2,1,0:T(8,128)}, bf16[64,4,512]{2,1,0:T(4,128)(2,1)}, bf16[64,4,4,64]{3,2,1,0:T(4,128)(2,1)}, bf16[64,4,4,64]{3,2,1,0:T(4,128)(2,...) custom-call(f32[64,4,64,64]{3,2,1,0:T(8,128)S(1)} %get-tuple-element.24.refs_0_, ...), custom_call_target="tpu_custom_call" | custom-call | tf_op jit(solution)/shard_map/finish/pallas_call | solution.py:773
